TPU v7x, 32 devices: a whole 2x2x4 slice. The times are simulated.
32 devices in a mesh: sp: 8 (over z, y), tp: 4 (over x, core).
Axes of the slice: x: 2, y: 2, z: 4, core: 2. Of those that a mesh axis runs over, the one named last changes fastest.
Arguments:
- residual_entry_input: bfloat16 [8192, 2048], P(('sp', 'tp')), may hold values from -6 to 6
- query_matrix_rows: bfloat16 [8192, 1024], P('sp', 'tp'), may hold values from -6 to 6
- key_matrix_rows: bfloat16 [8192, 1024], P('sp', 'tp'), may hold values from -6 to 6
- value_matrix_rows: bfloat16 [8192, 2048], P('sp', 'tp'), may hold values from -6 to 6
- output_gate_logits: bfloat16 [8192, 2048], P('sp', 'tp'), may hold values from -6 to 6
- input_gate_logits: float32 [8192, 8], P('sp', 'tp'), may hold values from -6 to 6
- forget_gate_logits: float32 [8192, 8], P('sp', 'tp'), may hold values from -8 to 31
- forget_decay_offset: float32 [8192, 8], P('sp', 'tp'), may hold values from -0.7 to 0
- head_norm_gain: float32 [8, 256], P('tp'), may hold values from 0.1 to 1.9
- cell_output_weight: bfloat16 [2048, 2048], P('tp'), may hold values from -0.125 to 0.125
- feedforward_norm_gain: float32 [2048], replicated, may hold values from 0.1 to 1.9
- gate_up_weight: bfloat16 [2048, 5632], P('sp', 'tp'), may hold values from -0.125 to 0.125
- value_up_weight: bfloat16 [2048, 5632], P('sp', 'tp'), may hold values from -0.125 to 0.125
- gate_filter_taps: float32 [3, 5632], P(None, 'tp'), may hold values from -3 to 3
- value_filter_taps: float32 [3, 5632], P(None, 'tp'), may hold values from -3 to 3
- down_projection_weight: bfloat16 [5632, 2048], P('tp', 'sp'), may hold values from -0.078125 to 0.078125
Outputs:
- result: bfloat16 [8192, 2048], P(('sp', 'tp'))
All inputs are finite; a program needn't handle non-finite values.
Results may differ from a plain program's by a relative error of at most 0.025.
Values may be sent and summed in bfloat16 or wider, within the bound.
A program may use at most 128 MiB of HBM per device.

v0:
```python
import jax
import jax.numpy as jnp
from jax import lax
from jax.sharding import PartitionSpec as P

BLOCK = 128


eps = 1e-06
neg_large = -1e30


def carried_in(x, axis, combine, identity):
    count, position = (lax.axis_size(axis), lax.axis_index(axis))
    everything = jax.tree.map(
        lambda part, kind: lax.all_gather(part.astype(kind), axis),
        x,
        (jnp.bfloat16, jnp.bfloat16, jnp.bfloat16, jnp.bfloat16),
    )
    start = jax.tree.map(
        lambda part, zero: jnp.broadcast_to(jnp.asarray(zero, part.dtype), part.shape), x, identity
    )

    def lap(k, before):
        reached = k < position
        new = combine(
            before, jax.tree.map(lambda part, own: part[k].astype(own.dtype), everything, x)
        )
        return jax.tree.map(lambda a, b: jnp.where(reached, a, b), new, before)

    return lax.fori_loop(0, count, lap, start)


def shifted(x, axis, by):
    count = lax.axis_size(axis)
    pairs = [(i, i + by) for i in range(count) if 0 <= i + by < count]
    return lax.ppermute(x, axis, pairs)


def gate_log_values(input_gate_logits, forget_gate_logits, forget_decay_offset):
    input_log_value = 15.0 * jnp.tanh(input_gate_logits / 15.0)
    forget_log_sigmoid = (
        jax.nn.log_sigmoid(15.0 * jnp.tanh(forget_gate_logits / 15.0)) + forget_decay_offset
    )
    return (input_log_value, forget_log_sigmoid)


def combine_states(earlier, later):
    total_one, memory_one, normer_one, running_one = earlier
    total_two, memory_two, normer_two, running_two = later
    joined = jnp.maximum(total_two + running_one, running_two)
    weight_one = jnp.exp(total_two + running_one - joined)
    weight_two = jnp.exp(running_two - joined)
    memory = weight_one[:, None, None] * memory_one + weight_two[:, None, None] * memory_two
    normer = weight_one[:, None] * normer_one + weight_two[:, None] * normer_two
    return (total_one + total_two, memory, normer, joined)


def local_step(state_carry, inputs):
    memory, normer, running = state_carry
    query_block, key_block, value_block, input_block, forget_block = inputs
    length = query_block.shape[0]
    highest = lax.Precision.HIGHEST
    query_scale = query_block.shape[2] ** (-0.5)
    causal = jnp.tril(jnp.ones((length, length), dtype=bool))[:, :, None]
    cumulative = jnp.cumsum(forget_block, axis=0)
    logits = cumulative[:, None, :] - cumulative[None, :, :] + input_block[None, :, :]
    logits = jnp.where(causal, logits, -jnp.inf)
    carried = cumulative + running[None, :]
    stable = jnp.maximum(carried, jnp.max(logits, axis=1))
    carry_weight = jnp.exp(carried - stable)
    raw = (
        jnp.einsum("thd,shd->tsh", query_block, key_block, preferred_element_type=jnp.float32)
        * query_scale
    )
    scores = raw * jnp.exp(logits - stable[:, None, :])
    scaled_query = query_block.astype(jnp.float32) * query_scale
    numerator = carry_weight[:, :, None] * jnp.einsum(
        "hvd,thd->thv", memory, scaled_query, precision=highest
    )
    numerator = numerator + jnp.einsum(
        "tsh,shv->thv", scores.astype(jnp.bfloat16), value_block, preferred_element_type=jnp.float32
    )
    denominator = carry_weight * jnp.einsum(
        "hd,thd->th", normer, scaled_query, precision=highest
    ) + jnp.sum(scores, axis=1)
    last_sum = cumulative[-1]
    weights_log = last_sum[None, :] - cumulative + input_block
    new_running = jnp.maximum(last_sum + running, jnp.max(weights_log, axis=0))
    decay_factor = jnp.exp(last_sum + running - new_running)
    weighted = (
        key_block.astype(jnp.float32) * jnp.exp(weights_log - new_running[None, :])[:, :, None]
    )
    memory = decay_factor[:, None, None] * memory + jnp.einsum(
        "shv,shd->hvd",
        value_block,
        weighted.astype(jnp.bfloat16),
        preferred_element_type=jnp.float32,
    )
    normer = decay_factor[:, None] * normer + jnp.sum(weighted, axis=0)
    return ((memory, normer, new_running), (numerator, denominator, stable))


def local(
    residual_entry_input,
    query_matrix_rows,
    key_matrix_rows,
    value_matrix_rows,
    output_gate_logits,
    input_gate_logits,
    forget_gate_logits,
    forget_decay_offset,
    head_norm_gain,
    cell_output_weight,
    feedforward_norm_gain,
    gate_up_weight,
    value_up_weight,
    gate_filter_taps,
    value_filter_taps,
    down_projection_weight,
):
    highest = lax.Precision.HIGHEST
    token_count = query_matrix_rows.shape[0]
    head_count = input_gate_logits.shape[1]
    key_width = query_matrix_rows.shape[1] // head_count
    value_width = value_matrix_rows.shape[1] // head_count
    query_scale = key_width ** (-0.5)
    queries_low = query_matrix_rows.reshape(token_count, head_count, key_width)
    keys_low = key_matrix_rows.reshape(token_count, head_count, key_width)
    values_low = value_matrix_rows.reshape(token_count, head_count, value_width)
    input_log_value, forget_log_sigmoid = gate_log_values(
        input_gate_logits, forget_gate_logits, forget_decay_offset
    )
    cumulative = jnp.cumsum(forget_log_sigmoid, axis=0)
    total_log = cumulative[-1]
    block_count = token_count // BLOCK

    def blocks(tensor):
        return tensor.reshape((block_count, BLOCK) + tensor.shape[1:])

    initial = (
        jnp.zeros((head_count, value_width, key_width), jnp.float32),
        jnp.zeros((head_count, key_width), jnp.float32),
        jnp.full((head_count,), neg_large, jnp.float32),
    )
    end_state, (numerator, denominator, stable) = lax.scan(
        local_step,
        initial,
        (
            blocks(queries_low),
            blocks(keys_low),
            blocks(values_low),
            blocks(input_log_value),
            blocks(forget_log_sigmoid),
        ),
    )
    end_memory, end_normer, end_running = end_state
    identity = (
        jnp.zeros((head_count,), jnp.float32),
        jnp.zeros((head_count, value_width, key_width), jnp.float32),
        jnp.zeros((head_count, key_width), jnp.float32),
        jnp.full((head_count,), neg_large, jnp.float32),
    )
    prefix = carried_in(
        (total_log, end_memory, end_normer, end_running), "sp", combine_states, identity
    )
    numerator = numerator.reshape(token_count, head_count, value_width)
    denominator = denominator.reshape(token_count, head_count)
    stable = stable.reshape(token_count, head_count)
    _, prior_memory, prior_normer, prior_running = prefix
    scaled_query = queries_low.astype(jnp.float32) * query_scale
    prior_log = cumulative + prior_running[None, :]
    top_log = jnp.maximum(stable, prior_log)
    local_weight = jnp.exp(stable - top_log)
    prior_weight = jnp.exp(prior_log - top_log)
    numerator = local_weight[:, :, None] * numerator + prior_weight[:, :, None] * jnp.einsum(
        "hvd,thd->thv", prior_memory, scaled_query, precision=highest
    )
    denominator = local_weight * denominator + prior_weight * jnp.einsum(
        "hd,thd->th", prior_normer, scaled_query, precision=highest
    )
    memory_out = numerator / jnp.maximum(jnp.abs(denominator), jnp.exp(-top_log))[:, :, None]
    normed = (
        memory_out
        * lax.rsqrt(jnp.mean(memory_out * memory_out, axis=-1, keepdims=True) + eps)
        * head_norm_gain[None, :, :]
    )
    gated_rows = (
        normed.reshape(token_count, head_count * value_width)
        * jax.nn.sigmoid(output_gate_logits.astype(jnp.float32))
    ).astype(jnp.bfloat16)
    whole_out = lax.all_gather(cell_output_weight, "tp", axis=0, tiled=True)
    own_rows = lax.all_to_all(gated_rows, "tp", split_axis=0, concat_axis=1, tiled=True)
    mixed_rows = jnp.dot(own_rows, whole_out, preferred_element_type=jnp.float32)
    stream_wide = residual_entry_input.astype(jnp.float32) + mixed_rows
    stream = stream_wide.astype(jnp.bfloat16)
    stream_wide = lax.optimization_barrier(stream).astype(jnp.float32)
    normed_rows = (
        stream_wide
        * lax.rsqrt(jnp.mean(stream_wide * stream_wide, axis=-1, keepdims=True) + eps)
        * feedforward_norm_gain[None, :]
    ).astype(jnp.bfloat16)
    group_rows = lax.all_gather(normed_rows, "tp", axis=0, tiled=True)
    earlier_rows = shifted(group_rows[-2:], "sp", 1)
    window = jnp.concatenate([earlier_rows, group_rows], axis=0)
    up_gate = jnp.dot(
        window,
        lax.all_gather(gate_up_weight, "sp", axis=0, tiled=True),
        preferred_element_type=jnp.float32,
    )
    up_value = jnp.dot(
        window,
        lax.all_gather(value_up_weight, "sp", axis=0, tiled=True),
        preferred_element_type=jnp.float32,
    )
    conv_g = (
        gate_filter_taps[0][None, :] * up_gate[:-2]
        + gate_filter_taps[1][None, :] * up_gate[1:-1]
        + gate_filter_taps[2][None, :] * up_gate[2:]
    )
    conv_v = (
        value_filter_taps[0][None, :] * up_value[:-2]
        + value_filter_taps[1][None, :] * up_value[1:-1]
        + value_filter_taps[2][None, :] * up_value[2:]
    )
    hidden = (jax.nn.silu(conv_g) * conv_v).astype(jnp.bfloat16)
    whole_down = lax.all_gather(down_projection_weight, "sp", axis=1, tiled=True)
    ffn_rows = lax.psum_scatter(
        jnp.dot(hidden, whole_down, preferred_element_type=jnp.float32).astype(jnp.bfloat16),
        "tp",
        scatter_dimension=0,
        tiled=True,
    ).astype(jnp.float32)
    return (stream_wide + ffn_rows).astype(jnp.bfloat16)


def solution(mesh):
    in_specs = (
        P(("sp", "tp"), None),
        P("sp", "tp"),
        P("sp", "tp"),
        P("sp", "tp"),
        P("sp", "tp"),
        P("sp", "tp"),
        P("sp", "tp"),
        P("sp", "tp"),
        P("tp", None),
        P("tp", None),
        P(),
        P("sp", "tp"),
        P("sp", "tp"),
        P(None, "tp"),
        P(None, "tp"),
        P("tp", "sp"),
    )
    out_specs = P(("sp", "tp"), None)
    return jax.shard_map(local, mesh=mesh, in_specs=in_specs, out_specs=out_specs, check_vma=False)
```

profile of v0, /device:TPU:29, one launch (start us, length us, event | category | flops | bytes accessed | tf_op | source)
XLA Modules:
  0.0 627.1 jit_solution(18224603662122398015)
XLA Ops:
  12.8 105.2 %while.39 = (s32[]{:T(128)}, f32[2,256,128]{2,1,0:T(8,128)S(1)}, f32[2,128]{1,0:T(2,128)S(1)}, f32[2]{0:T(128)S(1)}, f32[8,128,2,256]{1,0,3,2:T(8,128)}, /*index...) while((s32[]{:T(128)}, f32[2,256,128]{2,1,0:T(8,128)S(1)}, ...), condition=%wide.region_6.7_spmd.clone, body=%wide.region_0.6_spmd.clone.sunk | while | flops 144166400 | bytes 4685610 | solution.py:146
  17.3 8.2 %dynamic_update_slice.19 = f32[8,128,2,256]{1,0,3,2:T(8,128)} dynamic-update-slice(f32[8,128,2,256]{1,0,3,2:T(8,128)} %get-tuple-element.661, f32[1,128,2,256]{1,0,3,2:T(1,128)S(1)} %copy.248, s32[]{:T(128)} %get-tuple-element.657, s32[]{:T(128)} %constant.83.clone.1..sunk, s32[]{:T(128)} %constant.83.clone.1..sunk, s32[]{:T(128)} %constant.83.clone.1..sunk) | dynamic-update-slice | bytes 524292 | tf_op jit(solution)/shard_map/while/body/jit(dynamic_update_index_in_dim)/dynamic_update_slice | solution.py:146
  30.5 8.2 %dynamic_update_slice.19 = f32[8,128,2,256]{1,0,3,2:T(8,128)} dynamic-update-slice(f32[8,128,2,256]{1,0,3,2:T(8,128)} %get-tuple-element.661, f32[1,128,2,256]{1,0,3,2:T(1,128)S(1)} %copy.248, s32[]{:T(128)} %get-tuple-element.657, s32[]{:T(128)} %constant.83.clone.1..sunk, s32[]{:T(128)} %constant.83.clone.1..sunk, s32[]{:T(128)} %constant.83.clone.1..sunk) | dynamic-update-slice | bytes 524292 | tf_op jit(solution)/shard_map/while/body/jit(dynamic_update_index_in_dim)/dynamic_update_slice | solution.py:146
  43.7 8.2 %dynamic_update_slice.19 = f32[8,128,2,256]{1,0,3,2:T(8,128)} dynamic-update-slice(f32[8,128,2,256]{1,0,3,2:T(8,128)} %get-tuple-element.661, f32[1,128,2,256]{1,0,3,2:T(1,128)S(1)} %copy.248, s32[]{:T(128)} %get-tuple-element.657, s32[]{:T(128)} %constant.83.clone.1..sunk, s32[]{:T(128)} %constant.83.clone.1..sunk, s32[]{:T(128)} %constant.83.clone.1..sunk) | dynamic-update-slice | bytes 524292 | tf_op jit(solution)/shard_map/while/body/jit(dynamic_update_index_in_dim)/dynamic_update_slice | solution.py:146
  56.8 8.2 %dynamic_update_slice.19 = f32[8,128,2,256]{1,0,3,2:T(8,128)} dynamic-update-slice(f32[8,128,2,256]{1,0,3,2:T(8,128)} %get-tuple-element.661, f32[1,128,2,256]{1,0,3,2:T(1,128)S(1)} %copy.248, s32[]{:T(128)} %get-tuple-element.657, s32[]{:T(128)} %constant.83.clone.1..sunk, s32[]{:T(128)} %constant.83.clone.1..sunk, s32[]{:T(128)} %constant.83.clone.1..sunk) | dynamic-update-slice | bytes 524292 | tf_op jit(solution)/shard_map/while/body/jit(dynamic_update_index_in_dim)/dynamic_update_slice | solution.py:146
  70.0 8.2 %dynamic_update_slice.19 = f32[8,128,2,256]{1,0,3,2:T(8,128)} dynamic-update-slice(f32[8,128,2,256]{1,0,3,2:T(8,128)} %get-tuple-element.661, f32[1,128,2,256]{1,0,3,2:T(1,128)S(1)} %copy.248, s32[]{:T(128)} %get-tuple-element.657, s32[]{:T(128)} %constant.83.clone.1..sunk, s32[]{:T(128)} %constant.83.clone.1..sunk, s32[]{:T(128)} %constant.83.clone.1..sunk) | dynamic-update-slice | bytes 524292 | tf_op jit(solution)/shard_map/while/body/jit(dynamic_update_index_in_dim)/dynamic_update_slice | solution.py:146
  83.1 8.2 %dynamic_update_slice.19 = f32[8,128,2,256]{1,0,3,2:T(8,128)} dynamic-update-slice(f32[8,128,2,256]{1,0,3,2:T(8,128)} %get-tuple-element.661, f32[1,128,2,256]{1,0,3,2:T(1,128)S(1)} %copy.248, s32[]{:T(128)} %get-tuple-element.657, s32[]{:T(128)} %constant.83.clone.1..sunk, s32[]{:T(128)} %constant.83.clone.1..sunk, s32[]{:T(128)} %constant.83.clone.1..sunk) | dynamic-update-slice | bytes 524292 | tf_op jit(solution)/shard_map/while/body/jit(dynamic_update_index_in_dim)/dynamic_update_slice | solution.py:146
  96.3 8.2 %dynamic_update_slice.19 = f32[8,128,2,256]{1,0,3,2:T(8,128)} dynamic-update-slice(f32[8,128,2,256]{1,0,3,2:T(8,128)} %get-tuple-element.661, f32[1,128,2,256]{1,0,3,2:T(1,128)S(1)} %copy.248, s32[]{:T(128)} %get-tuple-element.657, s32[]{:T(128)} %constant.83.clone.1..sunk, s32[]{:T(128)} %constant.83.clone.1..sunk, s32[]{:T(128)} %constant.83.clone.1..sunk) | dynamic-update-slice | bytes 524292 | tf_op jit(solution)/shard_map/while/body/jit(dynamic_update_index_in_dim)/dynamic_update_slice | solution.py:146
  109.4 8.2 %dynamic_update_slice.19 = f32[8,128,2,256]{1,0,3,2:T(8,128)} dynamic-update-slice(f32[8,128,2,256]{1,0,3,2:T(8,128)} %get-tuple-element.661, f32[1,128,2,256]{1,0,3,2:T(1,128)S(1)} %copy.248, s32[]{:T(128)} %get-tuple-element.657, s32[]{:T(128)} %constant.83.clone.1..sunk, s32[]{:T(128)} %constant.83.clone.1..sunk, s32[]{:T(128)} %constant.83.clone.1..sunk) | dynamic-update-slice | bytes 524292 | tf_op jit(solution)/shard_map/while/body/jit(dynamic_update_index_in_dim)/dynamic_update_slice | solution.py:146
  122.2 12.6 %all-gather.3 = bf16[8,1,2]{2,1,0:T(2,128)(2,1)S(1)} all-gather(bf16[1,1,2]{2,1,0:T(2,128)(2,1)S(1)} %bitcast.273), channel_id=1, replica_groups=mesh['sp'=8,'tp'=4] {'sp'}, dimensions={0}, use_global_device_ids=true | all-gather | bytes 36 | tf_op jit(solution)/shard_map/all_gather | solution.py:16
  134.8 16.6 %all-reduce = bf16[16]{0:T(256)(128)(2,1)S(1)} all-reduce(bf16[16]{0:T(256)(128)(2,1)S(1)} %dynamic-update-slice), channel_id=2, replica_groups=mesh['sp'=8,'tp'=4] {'sp'}, use_global_device_ids=true, to_apply=%add | all-reduce | flops 16 | bytes 64
  155.8 12.6 %all-gather.4 = bf16[8,2,128]{2,1,0:T(2,128)(2,1)S(1)} all-gather(bf16[1,2,128]{2,1,0:T(2,128)(2,1)S(1)} %convert_bitcast_fusion), channel_id=4, replica_groups=mesh['sp'=8,'tp'=4] {'sp'}, dimensions={0}, use_global_device_ids=true | all-gather | bytes 4608 | tf_op jit(solution)/shard_map/all_gather | solution.py:16
  168.4 10.7 %while.40 = (s32[]{:T(128)}, f32[2,256,128]{2,1,0:T(8,128)S(1)}, f32[2,128]{1,0:T(2,128)S(1)}, f32[2]{0:T(128)S(1)}, s32[]{:T(128)}, /*index=5*/bf16[8,2]{0,1:T(...) while((s32[]{:T(128)}, f32[2,256,128]{2,1,0:T(8,128)S(1)}, ...), condition=%wide.region_10.11_spmd.clone, body=%wide.region_9.10_spmd.clone.sunk | while | flops 394772 | bytes 658157 | solution.py:31
  187.1 38.8 %all_to_all.19 = bf16[4,256,512]{2,1,0:T(8,128)(2,1)S(1)} all-to-all(bf16[4,256,512]{2,1,0:T(8,128)(2,1)S(1)} %bitcast.262), channel_id=1, replica_groups=mesh['sp'=8,'tp'=4] {'tp'}, dimensions={0} | all-to-all | bytes 2097152 | tf_op jit(solution)/shard_map/all_to_all | solution.py:193
  226.5 4.0 all-gather.12.cloned.1.call-done
  230.4 5.7 fusion.45
  239.8 32.6 %all-gather.14.cloned.1.call-done = bf16[1024,2048]{1,0:T(8,128)(2,1)} async-done(((bf16[256,2048]{1,0:T(8,128)(2,1)}), bf16[1024,2048]{1,0:T(8,128)(2,1)}) %all-gather.14.cloned.1.call-update) | async-done | bytes 4194320 | tf_op jit(solution)/shard_map/all_gather | solution.py:203
  274.6 89.0 %all-gather.16.cloned.1.call-done = bf16[2048,1408]{1,0:T(8,128)(2,1)} async-done(((bf16[256,1408]{1,0:T(8,128)(2,1)}), bf16[2048,1408]{1,0:T(8,128)(2,1)}) %all-gather.16.cloned.1.call-update) | async-done | bytes 5767184 | tf_op jit(solution)/shard_map/all_gather | solution.py:208
  363.6 11.9 %fusion.44 = f32[1026,1408]{1,0:T(8,128)} fusion(bf16[2048,1408]{1,0:T(8,128)(2,1)} %all-gather.16.cloned.1.call-done, bf16[1024,2048]{1,0:T(8,128)(2,1)} %all-gather.14.cloned.1.call-done, bf16[2,2048]{1,0:T(2,128)(2,1)S(1)} %collective-permute-done), kind=kOutput, calls=%fused_computation.90 | convolution fusion | flops 5925519360 | bytes 15748096 | tf_op jit(solution)/shard_map/dot_general | solution.py:206
  375.6 80.6 %all-gather.18.cloned.1.call-done = bf16[2048,1408]{1,0:T(8,128)(2,1)} async-done(((bf16[256,1408]{1,0:T(8,128)(2,1)}), bf16[2048,1408]{1,0:T(8,128)(2,1)}) %all-gather.18.cloned.1.call-update) | async-done | bytes 5767184 | tf_op jit(solution)/shard_map/all_gather | solution.py:213
  456.2 11.9 %fusion.43 = f32[1026,1408]{1,0:T(8,128)} fusion(bf16[2048,1408]{1,0:T(8,128)(2,1)} %all-gather.18.cloned.1.call-done, bf16[1024,2048]{1,0:T(8,128)(2,1)} %all-gather.14.cloned.1.call-done, bf16[2,2048]{1,0:T(2,128)(2,1)S(1)} %collective-permute-done), kind=kOutput, calls=%fused_computation.89 | convolution fusion | flops 5925519360 | bytes 15748096 | tf_op jit(solution)/shard_map/dot_general | solution.py:211
  468.1 81.3 %all-gather.20.cloned.1.call-done = bf16[1408,2048]{1,0:T(8,128)(2,1)} async-done(((bf16[1408,256]{1,0:T(8,128)(2,1)}), bf16[1408,2048]{1,0:T(8,128)(2,1)}) %all-gather.20.cloned.1.call-update) | async-done | bytes 5767184 | tf_op jit(solution)/shard_map/all_gather | solution.py:227
  549.4 22.7 %convolution_convert_fusion = bf16[1024,2048]{1,0:T(8,128)(2,1)} fusion(bf16[1408,2048]{1,0:T(8,128)(2,1)} %all-gather.20.cloned.1.call-done, f32[1026,1408]{1,0:T(8,128)} %fusion.43, f32[1026,1408]{1,0:T(8,128)} %fusion.44, f32[1408]{0:T(1024)S(1)} %get-tuple-element.403, f32[1408]{0:T(1024)S(1)} %get-tuple-element.404, f32[1408]{0:T(1024)S(1)} %get-tuple-element.402, ...), kind=kOutput, calls=%fused_computation.85 | convolution fusion | flops 5930745856 | bytes 44598272 | tf_op jit(solution)/shard_map/dot_general | solution.py:229
  572.1 45.5 %reduce-scatter.2.cloned.1.call-done = bf16[256,2048]{1,0:T(8,128)(2,1)} async-done(((bf16[1024,2048]{1,0:T(8,128)(2,1)}), bf16[256,2048]{1,0:T(8,128)(2,1)}) %reduce-scatter.2.cloned.1.call-update) | async-done | bytes 1048592 | tf_op jit(solution)/shard_map/reduce_scatter | solution.py:228
  (345 shorter events, 80.2 us)
Async XLA Ops:
  6.5 5.3 copy-start.1
  6.5 161.9 %all-gather.22.cloned.1.call-start = ((), (), s32[]{:S(2)}) async-start(), calls=%async_computation.8 | async-start | bytes 1179648 | tf_op jit(solution)/shard_map/all_gather | solution.py:16
  12.8 107.7 %copy-start.7 = (u32[32]{0:T(128)S(1)}, u32[32]{0:T(128)}, u32[]{:S(2)}) copy-start(u32[32]{0:T(128)} %constant.101) | copy-start | bytes 388
  118.7 111.7 %all-gather.12.cloned.1.call-start = ((), (), s32[]{:S(2)}) async-start(), calls=%async_computation.2 | async-start | bytes 10485760 | tf_op jit(solution)/shard_map/all_gather | solution.py:192
  119.4 153.0 %all-gather.14.cloned.1.call-start = ((), (), s32[]{:S(2)}) async-start(), calls=%async_computation.3 | async-start | bytes 5242880 | tf_op jit(solution)/shard_map/all_gather | solution.py:203
  152.8 26.3 %copy-start.2 = (bf16[1024,256]{1,0:T(8,128)(2,1)S(1)}, bf16[1024,256]{1,0:T(8,128)(2,1)}, u32[]{:S(2)}) copy-start(bf16[1024,256]{1,0:T(8,128)(2,1)} %param.21) | copy-start | bytes 1572868
  180.2 2.3 copy-start.6
  184.6 45.8 %copy-start = (bf16[256,2048]{1,0:T(8,128)(2,1)S(1)}, bf16[256,2048]{1,0:T(8,128)(2,1)}, u32[]{:S(2)}) copy-start(bf16[256,2048]{1,0:T(8,128)(2,1)} %param.20) | copy-start | bytes 3145732
  230.4 6.1 copy-start.5
  236.2 38.3 %copy-start.3 = (f32[3,1408]{1,0:T(4,128)S(1)}, f32[3,1408]{1,0:T(4,128)}, u32[]{:S(2)}) copy-start(f32[3,1408]{1,0:T(4,128)} %param.34) | copy-start | bytes 50692
  236.2 38.3 %copy-start.4 = (f32[3,1408]{1,0:T(4,128)S(1)}, f32[3,1408]{1,0:T(4,128)}, u32[]{:S(2)}) copy-start(f32[3,1408]{1,0:T(4,128)} %param.33) | copy-start | bytes 50692
  237.8 125.8 %all-gather.16.cloned.1.call-start = ((), (), s32[]{:S(2)}) async-start(), calls=%async_computation.4 | async-start | bytes 6488064 | tf_op jit(solution)/shard_map/all_gather | solution.py:208
  238.4 217.8 %all-gather.18.cloned.1.call-start = ((), (), s32[]{:S(2)}) async-start(), calls=%async_computation.5 | async-start | bytes 6488064 | tf_op jit(solution)/shard_map/all_gather | solution.py:213
  239.0 310.5 %all-gather.20.cloned.1.call-start = ((), (), s32[]{:S(2)}) async-start(), calls=%async_computation.6 | async-start | bytes 6488064 | tf_op jit(solution)/shard_map/all_gather | solution.py:227
  239.5 378.1 %reduce-scatter.2.cloned.1.call-start = ((), (), s32[]{:S(2)}) async-start(), calls=%async_computation.7 | async-start | bytes 5242880 | tf_op jit(solution)/shard_map/reduce_scatter | solution.py:228
  273.2 90.5 %collective-permute-start = (bf16[2,2048]{1,0:T(2,128)(2,1)S(1)}, bf16[2,2048]{1,0:T(2,128)(2,1)S(1)}, u32[]{:S(2)}, u32[]{:S(2)}) collective-permute-start(bf16[2,2048]{1,0:T(2,128)(2,1)S(1)} %slice.72), channel_id=1, source_target_pairs={{0,4},{4,8},{8,12},{12,16},{16,20},{20,24},{24,28},{1,5},{5,9},{9,... | collective-permute-start | bytes 24584 | tf_op jit(solution)/shard_map/ppermute | solution.py:37
Sparse Core Ops, SparseCore 0:
  118.8 37.2 all-gather.21
  157.6 72.7 all-gather.11
  237.9 34.4 all-gather.13
  274.5 89.1 all-gather.15
  365.7 90.4 all-gather.17
  458.1 91.3 all-gather.19
  572.2 45.3 reduce-scatter.1
where the time goes:
time: 631 us; the launch traced here: 627 us
  waiting for transfers between devices  335 us (53%)
  local copies, waits for them, and re-layouts  97.1 us (15%)
  blocking collectives  80.5 us (13%)
  matrix products  67.5 us (11%)
  other arithmetic  29.6 us (5%)
  between operations  14.4 us (2%)
    all_gather x1, waiting for transfers between devices, local(): lax.all_gather(gate_up_weight, 'sp', axis=0, tiled=True)  89 us
    all_gather x1, waiting for transfers between devices, local(): lax.all_gather(down_projection_weight, 'sp', axis=1, tiled=True)  81.3 us
    all_gather x1, waiting for transfers between devices, local(): lax.all_gather(value_up_weight, 'sp', axis=0, tiled=True)  80.6 us
    dynamic_update_slice x16, local copies, waits for them, and re-layouts, local(): lax.scan(local_step, initial, (blocks(queries_low), blocks(keys_low), blo...  66.7 us
    reduce_scatter x1, waiting for transfers between devices, local(): lax.psum_scatter(jnp.dot(hidden, whole_down, preferred_element_type=jnp.f...  45.5 us
    all_to_all x1, blocking collectives, local(): lax.all_to_all(gated_rows, 'tp', split_axis=0, concat_axis=1, tiled=True)  38.8 us
    all_gather x1, waiting for transfers between devices, local(): group_rows = lax.all_gather(normed_rows, 'tp', axis=0, tiled=True)  32.6 us
    all_gather x2, blocking collectives, carried_in(): lax.all_gather(part.astype(kind), axis)  25.1 us
  transfers between devices with their start and end apart: 8, of which 6 were waited for; matrix products, arithmetic and copies ran while one was open for 8% of the time, Pallas kernels for 0%

commit v1 on v0

v1 whole, which is shorter than its diff:
```python
import functools

import jax
import jax.numpy as jnp
from jax import lax
from jax.experimental import pallas as pl
from jax.experimental.pallas import tpu as pltpu
from jax.sharding import PartitionSpec as P

BLOCK = 128


eps = 1e-06
neg_large = -1e30


def shifted(x, axis, by):
    count = lax.axis_size(axis)
    pairs = [(i, i + by) for i in range(count) if 0 <= i + by < count]
    return lax.ppermute(x, axis, pairs)


def gate_log_values(input_gate_logits, forget_gate_logits, forget_decay_offset):
    input_log_value = 15.0 * jnp.tanh(input_gate_logits / 15.0)
    forget_log_sigmoid = (
        jax.nn.log_sigmoid(15.0 * jnp.tanh(forget_gate_logits / 15.0)) + forget_decay_offset
    )
    return (input_log_value, forget_log_sigmoid)


STATE_PAD = 16
MESH = pl.DeviceIdType.MESH


def cell_kernel(
    count,
    heads,
    state_ref,
    q_ref,
    k_ref,
    v_ref,
    gate_ref,
    gain_ref,
    rows_ref,
    cols_ref,
    out_ref,
    held,
    memory,
    normer,
    running,
    send_sem,
    recv_sem,
):
    me = lax.axis_index("sp")
    barrier = pltpu.get_barrier_semaphore()
    for d in range(1, count):
        pl.semaphore_signal(
            barrier, inc=1, device_id={"sp": lax.rem(me + d, count)}, device_id_type=MESH
        )
    pl.semaphore_wait(barrier, count - 1)

    def push(d, target, slot):
        return pltpu.make_async_remote_copy(
            src_ref=state_ref,
            dst_ref=held.at[slot],
            send_sem=send_sem.at[d],
            recv_sem=recv_sem.at[d],
            device_id={"sp": target},
            device_id_type=MESH,
        )

    for d in range(1, count):

        @pl.when(me + d < count)
        def _():
            push(d, me + d, me).start()

    memory[...] = jnp.zeros_like(memory)
    normer[...] = jnp.zeros_like(normer)
    running[...] = jnp.full(running.shape, neg_large, jnp.float32)
    for d in range(1, count):

        @pl.when(me - d >= 0)
        def _():
            push(d, lax.rem(me + d, count), me - d).wait_recv()

    key_width = memory.shape[1]
    value_width = memory.shape[2]
    span = key_width + STATE_PAD

    @pl.loop(0, me)
    def _(j):
        for h in range(heads):
            low = h * span
            extra = held[j, low + key_width : low + span, :].astype(jnp.float32)
            total = extra[2:3, :1] + extra[3:4, :1]
            level = extra[4:5, :1] + extra[5:6, :1]
            before = running[h, :1, :1]
            after = jnp.maximum(total + before, level)
            one = jnp.exp(total + before - after)
            two = jnp.exp(level - after)
            memory[h] = one * memory[h] + two * held[j, low : low + key_width, :].astype(
                jnp.float32
            )
            parts = extra[0:1, :key_width] + extra[1:2, :key_width]
            normer[h, :1, :] = one * normer[h, :1, :] + two * parts
            running[h] = jnp.broadcast_to(after, running.shape[1:])

    length = BLOCK
    scale = key_width ** (-0.5)
    at_row = lax.broadcasted_iota(jnp.int32, (length, length), 0)
    at_col = lax.broadcasted_iota(jnp.int32, (length, length), 1)
    causal = at_col <= at_row

    @pl.loop(0, q_ref.shape[0] // length)
    def _(j):
        rows = pl.ds(pl.multiple_of(j * length, length), length)
        lanes = rows_ref[j]
        cols = cols_ref[rows, :]
        for h in range(heads):
            keys = slice(h * key_width, (h + 1) * key_width)
            vals = slice(h * value_width, (h + 1) * value_width)
            q = q_ref[rows, keys]
            k = k_ref[rows, keys]
            v = v_ref[rows, vals]
            before = running[h, :1, :1]
            total = lanes[heads + h : heads + h + 1, :1]
            shifted_log = jnp.where(causal, lanes[h : h + 1, :], -jnp.inf)
            top = jnp.maximum(jnp.max(shifted_log, axis=1, keepdims=True), before)
            raw = (
                lax.dot_general(
                    q, k, (((1,), (1,)), ((), ())), preferred_element_type=jnp.float32
                )
                * scale
            )
            scores = raw * jnp.exp(shifted_log - top)
            carry = jnp.exp(before - top) * scale
            state = memory[h]
            high = state.astype(jnp.bfloat16)
            low = (state - high.astype(jnp.float32)).astype(jnp.bfloat16)
            carried = jnp.dot(q, high, preferred_element_type=jnp.float32) + jnp.dot(
                q, low, preferred_element_type=jnp.float32
            )
            numerator = carry * carried + jnp.dot(
                scores.astype(jnp.bfloat16), v, preferred_element_type=jnp.float32
            )
            denominator = carry * jnp.sum(
                q.astype(jnp.float32) * normer[h, :1, :], axis=1, keepdims=True
            ) + jnp.sum(scores, axis=1, keepdims=True)
            level = cols[:, h : h + 1] + top
            value = numerator / jnp.maximum(jnp.abs(denominator), jnp.exp(-level))
            mean = jnp.mean(value * value, axis=1, keepdims=True)
            normed = value * lax.rsqrt(mean + eps) * gain_ref[h : h + 1, :]
            gated = normed * jax.nn.sigmoid(gate_ref[rows, vals].astype(jnp.float32))
            out_ref[rows, vals] = gated.astype(out_ref.dtype)
            last = jnp.max(jnp.maximum(lanes[h : h + 1, :], before), axis=1, keepdims=True)
            decay = jnp.exp(before - last)
            weighted = k.astype(jnp.float32) * jnp.exp(cols[:, heads + h : heads + h + 1] - last)
            memory[h] = decay * state + lax.dot_general(
                weighted.astype(jnp.bfloat16),
                v,
                (((0,), (0,)), ((), ())),
                preferred_element_type=jnp.float32,
            )
            normer[h, :1, :] = decay * normer[h, :1, :] + jnp.sum(
                weighted, axis=0, keepdims=True
            )
            running[h] = jnp.broadcast_to(last + total, running.shape[1:])

    for d in range(1, count):

        @pl.when(me + d < count)
        def _():
            push(d, me + d, me).wait_send()


def halves(x):
    high = lax.reduce_precision(x, 8, 7)
    return (high.astype(jnp.bfloat16), (x - high).astype(jnp.bfloat16))


def cell(q, k, v, gates, input_log, forget_log, gain):
    heads = input_log.shape[1]
    tokens = q.shape[0]
    key_width = q.shape[1] // heads
    value_width = v.shape[1] // heads
    count = lax.axis_size("sp")
    blocks = tokens // BLOCK
    f = forget_log.reshape(blocks, BLOCK, heads)
    tri = jnp.tril(jnp.ones((BLOCK, BLOCK), jnp.float32))
    within = jnp.einsum("ts,bsh->bth", tri, f, precision=lax.Precision.HIGHEST)
    each = within[:, -1, :]
    later = jnp.triu(jnp.ones((blocks, blocks), jnp.float32), 1)
    after = jnp.einsum("bc,ch->bh", later, each, precision=lax.Precision.HIGHEST)
    total = jnp.sum(each, axis=0)
    shifted_log = input_log.reshape(blocks, BLOCK, heads) - within
    to_end = (shifted_log + (each + after)[:, None, :]).reshape(tokens, heads)
    level = jnp.max(to_end, axis=0)
    weighted = k.reshape(tokens, heads, key_width).astype(jnp.float32) * jnp.exp(to_end - level)[
        :, :, None
    ]
    memory = jnp.einsum(
        "shd,shv->hdv",
        weighted.astype(jnp.bfloat16),
        v.reshape(tokens, heads, value_width),
        preferred_element_type=jnp.float32,
    ).astype(jnp.bfloat16)
    normer = jnp.sum(weighted, axis=0)
    wide = (heads, 1, value_width)
    lines = [
        jnp.pad(part, ((0, 0), (0, value_width - key_width)))[:, None, :]
        for part in halves(normer)
    ]
    for scalar in (total, level):
        lines += [jnp.broadcast_to(part[:, None, None], wide) for part in halves(scalar)]
    lines.append(jnp.zeros((heads, STATE_PAD - len(lines), value_width), jnp.bfloat16))
    span = key_width + STATE_PAD
    state = jnp.concatenate([memory] + lines, axis=1).reshape(heads * span, value_width)
    lanes = jnp.concatenate(
        [
            jnp.transpose(shifted_log, (0, 2, 1)),
            jnp.broadcast_to(each[:, :, None], (blocks, heads, BLOCK)),
        ],
        axis=1,
    )
    cols = jnp.concatenate([within, shifted_log], axis=2).reshape(tokens, 2 * heads)
    vmem = pl.BlockSpec(memory_space=pltpu.VMEM)
    return pl.pallas_call(
        functools.partial(cell_kernel, count, heads),
        out_shape=jax.ShapeDtypeStruct(v.shape, jnp.bfloat16),
        in_specs=[vmem] * 8,
        out_specs=vmem,
        scratch_shapes=[
            pltpu.VMEM((count, heads * span, value_width), jnp.bfloat16),
            pltpu.VMEM((heads, key_width, value_width), jnp.float32),
            pltpu.VMEM((heads, 8, key_width), jnp.float32),
            pltpu.VMEM((heads, 8, 128), jnp.float32),
            pltpu.SemaphoreType.DMA((count,)),
            pltpu.SemaphoreType.DMA((count,)),
        ],
        compiler_params=pltpu.CompilerParams(
            collective_id=0, has_side_effects=True, vmem_limit_bytes=40 * 1024 * 1024
        ),
        cost_estimate=pl.CostEstimate(
            flops=30_000_000_000, bytes_accessed=8 * v.size, transcendentals=0
        ),
    )(state, q, k, v, gates, gain, lanes, cols)


def rows_kernel(pieces, x_ref, out_ref, own_sem, near_send, near_recv, far_send, far_recv, on_send, on_recv):
    me = lax.axis_index("tp")
    near = me + 1 - 2 * lax.rem(me, 2)
    far = lax.rem(me + 2, 4)
    opposite = lax.rem(near + 2, 4)
    size = x_ref.shape[0]
    step = size // pieces
    barrier = pltpu.get_barrier_semaphore()
    for other in (near, far):
        pl.semaphore_signal(barrier, inc=1, device_id={"tp": other}, device_id_type=MESH)
    pl.semaphore_wait(barrier, 2)

    def at(owner, p):
        return out_ref.at[pl.ds(pl.multiple_of(owner * size + p * step, step), step)]

    def send(src, dst, sems, p, target):
        return pltpu.make_async_remote_copy(
            src_ref=src,
            dst_ref=dst,
            send_sem=sems[0].at[p],
            recv_sem=sems[1].at[p],
            device_id={"tp": target},
            device_id_type=MESH,
        )

    mine = [x_ref.at[pl.ds(p * step, step)] for p in range(pieces)]
    far_out = [send(mine[p], at(me, p), (far_send, far_recv), p, far) for p in range(pieces)]
    near_out = [send(mine[p], at(me, p), (near_send, near_recv), p, near) for p in range(pieces)]
    far_in = [send(mine[p], at(far, p), (far_send, far_recv), p, far) for p in range(pieces)]
    near_in = [send(mine[p], at(near, p), (near_send, near_recv), p, near) for p in range(pieces)]
    onward = [send(at(far, p), at(far, p), (on_send, on_recv), p, near) for p in range(pieces)]
    on_in = [
        send(at(opposite, p), at(opposite, p), (on_send, on_recv), p, near)
        for p in range(pieces)
    ]
    for p in range(pieces):
        far_out[p].start()
    for p in range(pieces):
        near_out[p].start()
    whole = pl.ds(pl.multiple_of(me * size, size), size)
    own = pltpu.make_async_copy(x_ref, out_ref.at[whole], own_sem)
    own.start()
    for p in range(pieces):
        far_in[p].wait_recv()
        onward[p].start()
    own.wait()
    for p in range(pieces):
        near_in[p].wait_recv()
        on_in[p].wait_recv()
    for p in range(pieces):
        far_out[p].wait_send()
        near_out[p].wait_send()
        onward[p].wait_send()


def gather_rows(x):
    if lax.axis_size("tp") != 4:
        return lax.all_gather(x, "tp", axis=0, tiled=True)
    pieces = 4
    vmem = pl.BlockSpec(memory_space=pltpu.VMEM)
    return pl.pallas_call(
        functools.partial(rows_kernel, pieces),
        out_shape=jax.ShapeDtypeStruct((4 * x.shape[0], x.shape[1]), x.dtype),
        in_specs=[vmem],
        out_specs=vmem,
        scratch_shapes=[pltpu.SemaphoreType.DMA] + [pltpu.SemaphoreType.DMA((pieces,))] * 6,
        compiler_params=pltpu.CompilerParams(
            collective_id=1, has_side_effects=True, vmem_limit_bytes=16 * 1024 * 1024
        ),
        cost_estimate=pl.CostEstimate(
            flops=30_000_000_000, bytes_accessed=4 * x.size, transcendentals=0
        ),
    )(x)


def local(
    residual_entry_input,
    query_matrix_rows,
    key_matrix_rows,
    value_matrix_rows,
    output_gate_logits,
    input_gate_logits,
    forget_gate_logits,
    forget_decay_offset,
    head_norm_gain,
    cell_output_weight,
    feedforward_norm_gain,
    gate_up_weight,
    value_up_weight,
    gate_filter_taps,
    value_filter_taps,
    down_projection_weight,
):
    input_log, forget_log = gate_log_values(
        input_gate_logits, forget_gate_logits, forget_decay_offset
    )
    whole_gate = lax.all_gather(gate_up_weight, "sp", axis=0, tiled=True)
    whole_value = lax.all_gather(value_up_weight, "sp", axis=0, tiled=True)
    whole_down = lax.all_gather(down_projection_weight, "sp", axis=1, tiled=True)
    gated_rows = cell(
        query_matrix_rows,
        key_matrix_rows,
        value_matrix_rows,
        output_gate_logits,
        input_log,
        forget_log,
        head_norm_gain,
    )
    whole_out = lax.all_gather(cell_output_weight, "tp", axis=0, tiled=True)
    own_rows = lax.all_to_all(gated_rows, "tp", split_axis=0, concat_axis=1, tiled=True)
    mixed_rows = jnp.dot(own_rows, whole_out, preferred_element_type=jnp.float32)
    stream_wide = residual_entry_input.astype(jnp.float32) + mixed_rows
    stream = stream_wide.astype(jnp.bfloat16)
    stream_wide = lax.optimization_barrier(stream).astype(jnp.float32)
    normed_rows = (
        stream_wide
        * lax.rsqrt(jnp.mean(stream_wide * stream_wide, axis=-1, keepdims=True) + eps)
        * feedforward_norm_gain[None, :]
    ).astype(jnp.bfloat16)
    group_rows = gather_rows(normed_rows)
    earlier_rows = shifted(group_rows[-2:], "sp", 1)
    window = jnp.concatenate([earlier_rows, group_rows], axis=0)
    up_gate = jnp.dot(
        window,
        whole_gate,
        preferred_element_type=jnp.float32,
    )
    up_value = jnp.dot(
        window,
        whole_value,
        preferred_element_type=jnp.float32,
    )
    conv_g = (
        gate_filter_taps[0][None, :] * up_gate[:-2]
        + gate_filter_taps[1][None, :] * up_gate[1:-1]
        + gate_filter_taps[2][None, :] * up_gate[2:]
    )
    conv_v = (
        value_filter_taps[0][None, :] * up_value[:-2]
        + value_filter_taps[1][None, :] * up_value[1:-1]
        + value_filter_taps[2][None, :] * up_value[2:]
    )
    hidden = (jax.nn.silu(conv_g) * conv_v).astype(jnp.bfloat16)
    ffn_rows = lax.psum_scatter(
        jnp.dot(hidden, whole_down, preferred_element_type=jnp.float32).astype(jnp.bfloat16),
        "tp",
        scatter_dimension=0,
        tiled=True,
    ).astype(jnp.float32)
    return (stream_wide + ffn_rows).astype(jnp.bfloat16)


def solution(mesh):
    in_specs = (
        P(("sp", "tp"), None),
        P("sp", "tp"),
        P("sp", "tp"),
        P("sp", "tp"),
        P("sp", "tp"),
        P("sp", "tp"),
        P("sp", "tp"),
        P("sp", "tp"),
        P("tp", None),
        P("tp", None),
        P(),
        P("sp", "tp"),
        P("sp", "tp"),
        P(None, "tp"),
        P(None, "tp"),
        P("tp", "sp"),
    )
    out_specs = P(("sp", "tp"), None)
    return jax.shard_map(local, mesh=mesh, in_specs=in_specs, out_specs=out_specs, check_vma=False)
```

time: 631 us -> 435 us (0.69)
  local copies, waits for them, and re-layouts: 97.1 us -> 7.86 us
  waiting for transfers between devices: 335 us -> 265 us
  Pallas kernels: 0 us -> 64.9 us
  blocking collectives: 80.5 us -> 20.5 us
  other arithmetic: 29.6 us -> 6.51 us
  matrix products: 67.5 us -> 52.9 us
    all_gather x4 -> x2, waiting for transfers between devices: 202 us -> 135 us  [the longest x1 80.8 us: local(): whole_value = lax.all_gather(value_up_weight, 'sp', axis=0, tiled=True)]
    dynamic_update_slice x16 -> x0, local copies, waits for them, and re-layouts: 66.7 us -> none  [local(): lax.scan(local_step, initial, (blocks(queries_low), blocks(keys_low), blo...]
    pallas_call x0 -> x2, Pallas kernels: none -> 64.9 us  [the longest x1 38 us: cell(): pl.pallas_call(functools.partial(cell_kernel, count, heads), out_shape=ja...]
    all_gather x2 -> x0, blocking collectives: 25.1 us -> none  [carried_in(): lax.all_gather(part.astype(kind), axis)]
    all_to_all x1, blocking collectives: 38.8 us -> 20.5 us  [local(): lax.all_to_all(gated_rows, 'tp', split_axis=0, concat_axis=1, tiled=True)]
    unnamed x1 -> x0, blocking collectives: 16.6 us -> none
    dot_general x44 -> x5, matrix products: 39.1 us -> 24.4 us  [the longest x1 11.9 us: local(): up_gate = jnp.dot(window, whole_gate, preferred_element_type=jnp.float32)]
    dynamic_slice x40 -> x0, local copies, waits for them, and re-layouts: 11.3 us -> none  [the longest x24 9.87 us: local(): lax.scan(local_step, initial, (blocks(queries_low), blocks(keys_low), blo...]
  transfers between devices with their start and end apart: 8 -> 6, of which waited for: 6 -> 4; matrix products, arithmetic and copies ran while one was open for 8% -> 9% of each run, Pallas kernels for 0% -> 15%
where the time goes in v1:
time: 435 us; the launch traced here: 432 us
  waiting for transfers between devices  265 us (61%)
  Pallas kernels  64.9 us (15%)
  matrix products  52.9 us (12%)
  blocking collectives  20.5 us (5%)
  between operations  13.4 us (3%)
  local copies, waits for them, and re-layouts  7.86 us (2%)
  other arithmetic  6.51 us (1%)
    all_gather x1, waiting for transfers between devices, local(): lax.all_gather(down_projection_weight, 'sp', axis=1, tiled=True)  81.4 us
    all_gather x1, waiting for transfers between devices, local(): whole_value = lax.all_gather(value_up_weight, 'sp', axis=0, tiled=True)  80.8 us
    all_gather x1, waiting for transfers between devices, local(): whole_gate = lax.all_gather(gate_up_weight, 'sp', axis=0, tiled=True)  54.5 us
    reduce_scatter x1, waiting for transfers between devices, local(): lax.psum_scatter(jnp.dot(hidden, whole_down, preferred_element_type=jnp.f...  45.5 us
    pallas_call x1, Pallas kernels, cell(): pl.pallas_call(functools.partial(cell_kernel, count, heads), out_shape=ja...  38 us
    pallas_call x1, Pallas kernels, gather_rows(): pl.pallas_call(functools.partial(rows_kernel, pieces), out_shape=jax.Shap...  26.9 us
    dot_general x1, matrix products, local(): jnp.dot(hidden, whole_down, preferred_element_type=jnp.float32)  22.5 us
    all_to_all x1, blocking collectives, local(): lax.all_to_all(gated_rows, 'tp', split_axis=0, concat_axis=1, tiled=True)  20.5 us
  transfers between devices with their start and end apart: 6, of which 4 were waited for; matrix products, arithmetic and copies ran while one was open for 9% of the time, Pallas kernels for 15%

profile of v1, /device:TPU:29, one launch (start us, length us, event | category | flops | bytes accessed | tf_op | source)
XLA Modules:
  0.0 432.4 jit_solution(3339959249675511386)
XLA Ops:
  6.5 0.7 all-gather.5.cloned.1.call-update
  7.3 0.7 all-gather.7.cloned.1.call-update
  8.1 0.7 all-gather.9.cloned.1.call-update
  9.4 0.7 fusion.24
  10.9 0.9 add_reduce_fusion
  12.0 1.3 copy.48
  13.5 1.4 multiply_reduce_fusion
  16.2 1.3 copy-done.3
  17.6 1.1 copy-done.4
  18.7 38.0 %shard_map.154 = bf16[1024,512]{1,0:T(8,128)(2,1)S(1)} custom-call(bf16[288,256]{1,0:T(8,128)(2,1)S(1)} %bitcast.54, bf16[1024,256]{1,0:T(8,128)(2,1)S(1)} %copy-done.4, bf16[1024,256]{1,0:T(8,128)(2,1)S(1)} %copy-done, bf16[1024,512]{1,0:T(8,128)(2,1)S(1)} %copy-done.1, bf16[1024,512]{1,0:T(8,128)(2,1)S(1)} %copy-done.3, f32[2,256]{1,0:T(2,128)S(1)} %copy-done.5, ...), custom_call_target="tpu_custom_call" | custom-call | flops 30000001024 | bytes 4194304 | tf_op jit(solution)/shard_map/pallas_call | solution.py:228
  56.7 0.5 copy.46
  57.2 20.5 %all_to_all.19 = bf16[4,256,512]{1,2,0:T(8,128)(2,1)S(1)} all-to-all(bf16[4,256,512]{1,2,0:T(8,128)(2,1)S(1)} %copy.46), channel_id=1, replica_groups=mesh['sp'=8,'tp'=4] {'tp'}, dimensions={0} | all-to-all | bytes 2097152 | tf_op jit(solution)/shard_map/all_to_all | solution.py:359
  77.7 6.0 %fusion.9 = bf16[256,2048]{1,0:T(8,128)(2,1)S(1)} fusion(bf16[256,2048]{0,1:T(8,128)(2,1)S(1)} %bitcast.55, bf16[2048,2048]{1,0:T(8,128)(2,1)} %all-gather.5.cloned.1.call-done, bf16[256,2048]{1,0:T(8,128)(2,1)} %param.16), kind=kOutput, calls=%fused_computation.20 | convolution fusion | flops 2149056512 | bytes 11534336 | tf_op jit(solution)/shard_map/dot_general | solution.py:360
  84.3 26.9 %shard_map.155 = bf16[1024,2048]{1,0:T(8,128)(2,1)S(1)} custom-call(bf16[256,2048]{1,0:T(8,128)(2,1)S(1)} %fusion.12.x_ref), custom_call_target="tpu_custom_call" | custom-call | flops 30000001024 | bytes 2097152 | tf_op jit(solution)/shard_map/pallas_call | solution.py:310
  111.2 2.0 copy-done.2
  113.2 1.5 collective-permute-start
  114.8 54.5 %all-gather.7.cloned.1.call-done = bf16[2048,1408]{1,0:T(8,128)(2,1)} async-done(((bf16[256,1408]{1,0:T(8,128)(2,1)}), bf16[2048,1408]{1,0:T(8,128)(2,1)}) %all-gather.7.cloned.1.call-update) | async-done | bytes 5767184 | tf_op jit(solution)/shard_map/all_gather | solution.py:346
  169.3 11.9 %fusion.8 = f32[1026,1408]{1,0:T(8,128)} fusion(bf16[2048,1408]{1,0:T(8,128)(2,1)} %all-gather.7.cloned.1.call-done, bf16[1024,2048]{1,0:T(8,128)(2,1)} %copy-done.2, bf16[2,2048]{1,0:T(2,128)(2,1)S(1)} %collective-permute-done), kind=kOutput, calls=%fused_computation.18 | convolution fusion | flops 5925519360 | bytes 15748096 | tf_op jit(solution)/shard_map/dot_general | solution.py:372
  181.3 80.8 %all-gather.9.cloned.1.call-done = bf16[2048,1408]{1,0:T(8,128)(2,1)} async-done(((bf16[256,1408]{1,0:T(8,128)(2,1)}), bf16[2048,1408]{1,0:T(8,128)(2,1)}) %all-gather.9.cloned.1.call-update) | async-done | bytes 5767184 | tf_op jit(solution)/shard_map/all_gather | solution.py:347
  262.1 11.8 %fusion.7 = f32[1026,1408]{1,0:T(8,128)} fusion(bf16[2048,1408]{1,0:T(8,128)(2,1)} %all-gather.9.cloned.1.call-done, bf16[1024,2048]{1,0:T(8,128)(2,1)} %copy-done.2, bf16[2,2048]{1,0:T(2,128)(2,1)S(1)} %collective-permute-done), kind=kOutput, calls=%fused_computation.17 | convolution fusion | flops 5925519360 | bytes 15748096 | tf_op jit(solution)/shard_map/dot_general | solution.py:377
  273.9 81.4 %all-gather.11.cloned.1.call-done = bf16[1408,2048]{1,0:T(8,128)(2,1)} async-done(((bf16[1408,256]{1,0:T(8,128)(2,1)}), bf16[1408,2048]{1,0:T(8,128)(2,1)}) %all-gather.11.cloned.1.call-update) | async-done | bytes 5767184 | tf_op jit(solution)/shard_map/all_gather | solution.py:348
  355.3 22.5 %convolution_convert_fusion = bf16[1024,2048]{1,0:T(8,128)(2,1)} fusion(bf16[1408,2048]{1,0:T(8,128)(2,1)} %all-gather.11.cloned.1.call-done, f32[1026,1408]{1,0:T(8,128)} %fusion.7, f32[1026,1408]{1,0:T(8,128)} %fusion.8, f32[1408]{0:T(1024)S(1)} %get-tuple-element.9, f32[1408]{0:T(1024)S(1)} %get-tuple-element.10, f32[1408]{0:T(1024)S(1)} %get-tuple-element.8, ...), kind=kOutput, calls=%fused_computation.13 | convolution fusion | flops 5930745856 | bytes 44598272 | tf_op jit(solution)/shard_map/dot_general | solution.py:394
  377.9 45.5 %reduce-scatter.2.cloned.1.call-done = bf16[256,2048]{1,0:T(8,128)(2,1)} async-done(((bf16[1024,2048]{1,0:T(8,128)(2,1)}), bf16[256,2048]{1,0:T(8,128)(2,1)}) %reduce-scatter.2.cloned.1.call-update) | async-done | bytes 1048592 | tf_op jit(solution)/shard_map/reduce_scatter | solution.py:393
  423.4 2.5 fusion.13
  (56 shorter events, 3.8 us)
Async XLA Ops:
  6.5 6.8 %copy-start = (bf16[1024,256]{1,0:T(8,128)(2,1)S(1)}, bf16[1024,256]{1,0:T(8,128)(2,1)}, u32[]{:S(2)}) copy-start(bf16[1024,256]{1,0:T(8,128)(2,1)} %k_ref.1) | copy-start | bytes 1572868
  6.5 8.8 %copy-start.1 = (bf16[1024,512]{1,0:T(8,128)(2,1)S(1)}, bf16[1024,512]{1,0:T(8,128)(2,1)}, u32[]{:S(2)}) copy-start(bf16[1024,512]{1,0:T(8,128)(2,1)} %v_ref.1) | copy-start | bytes 3145732
  6.5 71.2 %all-gather.5.cloned.1.call-start = ((), (), s32[]{:S(2)}) async-start(), calls=%async_computation.2 | async-start | bytes 10485760 | tf_op jit(solution)/shard_map/all_gather | solution.py:358
  7.3 9.0 %copy-start.5 = (f32[2,256]{1,0:T(2,128)S(1)}, f32[2,256]{1,0:T(2,128)}, u32[]{:S(2)}) copy-start(f32[2,256]{1,0:T(2,128)} %gain_ref.1) | copy-start | bytes 6148
  7.3 162.1 %all-gather.7.cloned.1.call-start = ((), (), s32[]{:S(2)}) async-start(), calls=%async_computation.3 | async-start | bytes 6488064 | tf_op jit(solution)/shard_map/all_gather | solution.py:346
  8.0 254.0 %all-gather.9.cloned.1.call-start = ((), (), s32[]{:S(2)}) async-start(), calls=%async_computation.4 | async-start | bytes 6488064 | tf_op jit(solution)/shard_map/all_gather | solution.py:347
  8.8 346.6 %all-gather.11.cloned.1.call-start = ((), (), s32[]{:S(2)}) async-start(), calls=%async_computation.5 | async-start | bytes 6488064 | tf_op jit(solution)/shard_map/all_gather | solution.py:348
  9.3 414.0 %reduce-scatter.2.cloned.1.call-start = ((), (), s32[]{:S(2)}) async-start(), calls=%async_computation.6 | async-start | bytes 5242880 | tf_op jit(solution)/shard_map/reduce_scatter | solution.py:393
  16.2 1.4 copy-start.3
  17.6 1.1 copy-start.4
  77.7 6.3 %copy-start.8 = (f32[2048]{0:T(1024)S(1)}, f32[2048]{0:T(1024)}, u32[]{:S(2)}) copy-start(f32[2048]{0:T(1024)} %param.26) | copy-start | bytes 24580
  84.3 30.4 %copy-start.6 = (f32[3,1408]{1,0:T(4,128)S(1)}, f32[3,1408]{1,0:T(4,128)}, u32[]{:S(2)}) copy-start(f32[3,1408]{1,0:T(4,128)} %param.30) | copy-start | bytes 50692
  84.3 30.4 %copy-start.7 = (f32[3,1408]{1,0:T(4,128)S(1)}, f32[3,1408]{1,0:T(4,128)}, u32[]{:S(2)}) copy-start(f32[3,1408]{1,0:T(4,128)} %param.29) | copy-start | bytes 50692
  111.2 2.0 copy-start.2
  113.2 56.1 %collective-permute-start = (bf16[2,2048]{1,0:T(2,128)(2,1)S(1)}, bf16[2,2048]{1,0:T(2,128)(2,1)S(1)}, u32[]{:S(2)}, u32[]{:S(2)}) collective-permute-start(bf16[2,2048]{1,0:T(2,128)(2,1)S(1)} %slice.44), channel_id=1, source_target_pairs={{0,4},{4,8},{8,12},{12,16},{16,20},{20,24},{24,28},{1,5},{5,9},{9,... | collective-permute-start | bytes 24584 | tf_op jit(solution)/shard_map/ppermute | solution.py:20
Sparse Core Ops, SparseCore 0:
  8.9 62.1 all-gather.4
  73.3 96.0 all-gather.6
  171.5 90.4 all-gather.8
  264.0 91.3 all-gather.10
  378.0 45.3 reduce-scatter.1

commit v2 on v1

--- a/solution.py
+++ b/solution.py
@@ -322,6 +322,118 @@
     )(x)
 
 
+def product_kernel(
+    pieces,
+    x_ref,
+    w_ref,
+    out_ref,
+    pair_out,
+    pair_in,
+    far_out,
+    far_in,
+    near_out,
+    near_in,
+    pair_send,
+    pair_recv,
+    far_send,
+    far_recv,
+    near_send,
+    near_recv,
+):
+    me = lax.axis_index("tp")
+    near = me + 1 - 2 * lax.rem(me, 2)
+    far = lax.rem(me + 2, 4)
+    opposite = lax.rem(near + 2, 4)
+    size = out_ref.shape[0]
+    step = out_ref.shape[1] // pieces
+    barrier = pltpu.get_barrier_semaphore()
+    for other in (near, far):
+        pl.semaphore_signal(barrier, inc=1, device_id={"tp": other}, device_id_type=MESH)
+    pl.semaphore_wait(barrier, 2)
+
+    def columns(p):
+        return pl.ds(pl.multiple_of(p * step, step), step)
+
+    def term(owner, p):
+        rows = pl.ds(pl.multiple_of(owner * size, size), size)
+        return jnp.dot(x_ref[rows, :], w_ref[:, columns(p)], preferred_element_type=jnp.float32)
+
+    def send(src, dst, sems, p, target):
+        return pltpu.make_async_remote_copy(
+            src_ref=src.at[p],
+            dst_ref=dst.at[p],
+            send_sem=sems[0].at[p],
+            recv_sem=sems[1].at[p],
+            device_id={"tp": target},
+            device_id_type=MESH,
+        )
+
+    def pair(p):
+        return send(pair_out, pair_in, (pair_send, pair_recv), p, near)
+
+    def across(p):
+        return send(far_out, far_in, (far_send, far_recv), p, far)
+
+    def beside(p):
+        return send(near_out, near_in, (near_send, near_recv), p, near)
+
+    @pl.loop(0, pieces)
+    def _(p):
+        pair_out[p] = term(opposite, p).astype(jnp.bfloat16)
+        pair(p).start()
+        mine = term(far, p)
+        pair(p).wait_recv()
+        far_out[p] = (mine + pair_in[p].astype(jnp.float32)).astype(jnp.bfloat16)
+        across(p).start()
+
+    @pl.loop(0, pieces)
+    def _(p):
+        near_out[p] = term(near, p).astype(jnp.bfloat16)
+        beside(p).start()
+
+    @pl.loop(0, pieces)
+    def _(p):
+        own = term(me, p)
+        beside(p).wait_recv()
+        out_ref[:, columns(p)] = own + near_in[p].astype(jnp.float32)
+
+    @pl.loop(0, pieces)
+    def _(p):
+        across(p).wait_recv()
+        out_ref[:, columns(p)] += far_in[p].astype(jnp.float32)
+
+    @pl.loop(0, pieces)
+    def _(p):
+        pair(p).wait_send()
+        across(p).wait_send()
+        beside(p).wait_send()
+
+
+def product_rows(x, w, tag):
+    if lax.axis_size("tp") != 4:
+        partial = jnp.dot(x, w, preferred_element_type=jnp.float32).astype(jnp.bfloat16)
+        return lax.psum_scatter(partial, "tp", scatter_dimension=0, tiled=True).astype(
+            jnp.float32
+        )
+    pieces = 4
+    rows, wide = x.shape[0] // 4, w.shape[1]
+    vmem = pl.BlockSpec(memory_space=pltpu.VMEM)
+    slots = pltpu.VMEM((pieces, rows, wide // pieces), jnp.bfloat16)
+    return pl.pallas_call(
+        functools.partial(product_kernel, pieces),
+        out_shape=jax.ShapeDtypeStruct((rows, wide), jnp.float32),
+        in_specs=[vmem] * 2,
+        out_specs=vmem,
+        scratch_shapes=[slots] * 6 + [pltpu.SemaphoreType.DMA((pieces,))] * 6,
+        compiler_params=pltpu.CompilerParams(
+            collective_id=tag, has_side_effects=True, vmem_limit_bytes=40 * 1024 * 1024
+        ),
+        cost_estimate=pl.CostEstimate(
+            flops=30_000_000_000, bytes_accessed=2 * w.size, transcendentals=0
+        ),
+    )(x, w)
+
+
 def local(
     residual_entry_input,
     query_matrix_rows,
@@ -355,9 +467,7 @@
         forget_log,
         head_norm_gain,
     )
-    whole_out = lax.all_gather(cell_output_weight, "tp", axis=0, tiled=True)
-    own_rows = lax.all_to_all(gated_rows, "tp", split_axis=0, concat_axis=1, tiled=True)
-    mixed_rows = jnp.dot(own_rows, whole_out, preferred_element_type=jnp.float32)
+    mixed_rows = product_rows(gated_rows, cell_output_weight, 2)
     stream_wide = residual_entry_input.astype(jnp.float32) + mixed_rows
     stream = stream_wide.astype(jnp.bfloat16)
     stream_wide = lax.optimization_barrier(stream).astype(jnp.float32)
@@ -390,12 +500,7 @@
         + value_filter_taps[2][None, :] * up_value[2:]
     )
     hidden = (jax.nn.silu(conv_g) * conv_v).astype(jnp.bfloat16)
-    ffn_rows = lax.psum_scatter(
-        jnp.dot(hidden, whole_down, preferred_element_type=jnp.float32).astype(jnp.bfloat16),
-        "tp",
-        scatter_dimension=0,
-        tiled=True,
-    ).astype(jnp.float32)
+    ffn_rows = product_rows(hidden, whole_down, 3)
     return (stream_wide + ffn_rows).astype(jnp.bfloat16)
 
 

time: 435 us -> 352 us (0.81)
  waiting for transfers between devices: 265 us -> 144 us
  Pallas kernels: 64.9 us -> 143 us
  matrix products: 52.9 us -> 24.5 us
  blocking collectives: 20.5 us -> 0 us
    pallas_call x0 -> x2, Pallas kernels: none -> 56.1 us  [product_rows(): pl.pallas_call(functools.partial(product_kernel, pieces), out_shape=jax.S...]
    all_gather x1, waiting for transfers between devices: 54.5 us -> 0.01 us  [local(): whole_gate = lax.all_gather(gate_up_weight, 'sp', axis=0, tiled=True)]
    reduce_scatter x1 -> x0, waiting for transfers between devices: 45.5 us -> none  [local(): lax.psum_scatter(jnp.dot(hidden, whole_down, preferred_element_type=jnp.f...]
    dot_general x2 -> x0, matrix products: 28.5 us -> none  [the longest x1 22.5 us: local(): jnp.dot(hidden, whole_down, preferred_element_type=jnp.float32)]
    all_gather x1, waiting for transfers between devices: 80.8 us -> 60.3 us  [local(): whole_value = lax.all_gather(value_up_weight, 'sp', axis=0, tiled=True)]
    all_to_all x1 -> x0, blocking collectives: 20.5 us -> none  [local(): lax.all_to_all(gated_rows, 'tp', split_axis=0, concat_axis=1, tiled=True)]
    pallas_call x1, Pallas kernels: 38 us -> 57.5 us  [cell(): pl.pallas_call(functools.partial(cell_kernel, count, heads), out_shape=ja...]
    convert_element_type x0 -> x2, other arithmetic: none -> 5.03 us  [the longest x1 4.75 us: local(): hidden = (jax.nn.silu(conv_g) * conv_v).astype(jnp.bfloat16)]
  transfers between devices with their start and end apart: 6 -> 4, of which waited for: 4 -> 3; matrix products, arithmetic and copies ran while one was open for 9% -> 12% of each run, Pallas kernels for 15% -> 33%
where the time goes in v2:
time: 352 us; the launch traced here: 348 us
  waiting for transfers between devices  144 us (41%)
  Pallas kernels  143 us (41%)
  matrix products  24.5 us (7%)
  between operations  13.4 us (4%)
  local copies, waits for them, and re-layouts  11.2 us (3%)
  other arithmetic  10.3 us (3%)
    all_gather x1, waiting for transfers between devices, local(): lax.all_gather(down_projection_weight, 'sp', axis=1, tiled=True)  77.9 us
    all_gather x1, waiting for transfers between devices, local(): whole_value = lax.all_gather(value_up_weight, 'sp', axis=0, tiled=True)  60.3 us
    pallas_call x1, Pallas kernels, cell(): pl.pallas_call(functools.partial(cell_kernel, count, heads), out_shape=ja...  57.5 us
    pallas_call x2, Pallas kernels, product_rows(): pl.pallas_call(functools.partial(product_kernel, pieces), out_shape=jax.S...  56.1 us
    pallas_call x1, Pallas kernels, gather_rows(): pl.pallas_call(functools.partial(rows_kernel, pieces), out_shape=jax.Shap...  29 us
    dot_general x1, matrix products, local(): up_gate = jnp.dot(window, whole_gate, preferred_element_type=jnp.float32)  11.9 us
    dot_general x1, matrix products, local(): up_value = jnp.dot(window, whole_value, preferred_element_type=jnp.float32)  10.7 us
  transfers between devices with their start and end apart: 4, of which 3 were waited for; matrix products, arithmetic and copies ran while one was open for 12% of the time, Pallas kernels for 33%

profile of v2, /device:TPU:29, one launch (start us, length us, event | category | flops | bytes accessed | tf_op | source)
XLA Modules:
  0.0 347.5 jit_solution(5558940217011586837)
XLA Ops:
  6.6 0.7 all-gather.4.cloned.1.call-update
  7.3 0.7 all-gather.6.cloned.1.call-update
  8.8 0.7 fusion.22
  10.2 0.9 add_reduce_fusion
  11.3 1.1 mul.107
  12.4 2.5 copy.46
  14.9 1.2 copy.45
  16.1 1.4 multiply_reduce_fusion
  17.8 1.6 convolution_convert_fusion
  20.1 1.1 copy-done.5
  21.2 57.5 %shard_map.154.x_ref = bf16[1024,512]{1,0:T(8,128)(2,1)S(1)} custom-call(bf16[288,256]{1,0:T(8,128)(2,1)S(1)} %bitcast.46, bf16[1024,256]{1,0:T(8,128)(2,1)S(1)} %copy-done.5, bf16[1024,256]{1,0:T(8,128)(2,1)S(1)} %copy-done, bf16[1024,512]{1,0:T(8,128)(2,1)S(1)} %copy-done.1, bf16[1024,512]{1,0:T(8,128)(2,1)S(1)} %copy-done.4, f32[2,256]{1,0:T(2,128)S(1)} %copy-done.6, ...), custom_call_target="tpu_custom_call" | custom-call | flops 30000001024 | bytes 4194304 | tf_op jit(solution)/shard_map/pallas_call | solution.py:228
  78.8 27.7 %shard_map.155 = f32[256,2048]{1,0:T(8,128)S(1)} custom-call(bf16[1024,512]{1,0:T(8,128)(2,1)S(1)} %shard_map.154.x_ref, bf16[512,2048]{1,0:T(8,128)(2,1)S(1)} %copy-done.3), custom_call_target="tpu_custom_call" | custom-call | flops 30000001024 | bytes 2097152 | tf_op jit(solution)/shard_map/pallas_call | solution.py:422
  108.1 29.0 %shard_map.156 = bf16[1024,2048]{1,0:T(8,128)(2,1)} custom-call(bf16[256,2048]{1,0:T(8,128)(2,1)S(1)} %fusion.10.x_ref), custom_call_target="tpu_custom_call" | custom-call | flops 30000001024 | bytes 2097152 | tf_op jit(solution)/shard_map/pallas_call | solution.py:310
  137.2 0.8 slice.44
  138.0 1.5 collective-permute-start
  139.6 3.5 %collective-permute-done = bf16[2,2048]{1,0:T(2,128)(2,1)S(1)} collective-permute-done((bf16[2,2048]{1,0:T(2,128)(2,1)S(1)}, bf16[2,2048]{1,0:T(2,128)(2,1)S(1)}, u32[]{:S(2)}, u32[]{:S(2)}) %collective-permute-start) | collective-permute-done | bytes 8224 | tf_op jit(solution)/shard_map/ppermute | solution.py:20
  143.1 11.9 %fusion.7 = f32[1026,1408]{1,0:T(8,128)} fusion(bf16[2048,1408]{1,0:T(8,128)(2,1)} %all-gather.4.cloned.1.call-done, bf16[1024,2048]{1,0:T(8,128)(2,1)} %shard_map.156, bf16[2,2048]{1,0:T(2,128)(2,1)S(1)} %collective-permute-done), kind=kOutput, calls=%fused_computation.17 | convolution fusion | flops 5925519360 | bytes 15748096 | tf_op jit(solution)/shard_map/dot_general | solution.py:482
  155.0 60.3 %all-gather.6.cloned.1.call-done = bf16[2048,1408]{1,0:T(8,128)(2,1)} async-done(((bf16[256,1408]{1,0:T(8,128)(2,1)}), bf16[2048,1408]{1,0:T(8,128)(2,1)}) %all-gather.6.cloned.1.call-update) | async-done | bytes 5767184 | tf_op jit(solution)/shard_map/all_gather | solution.py:459
  215.3 10.7 %fusion.6 = f32[1026,1408]{1,0:T(8,128)S(1)} fusion(bf16[2048,1408]{1,0:T(8,128)(2,1)} %all-gather.6.cloned.1.call-done, bf16[1024,2048]{1,0:T(8,128)(2,1)} %shard_map.156, bf16[2,2048]{1,0:T(2,128)(2,1)S(1)} %collective-permute-done), kind=kOutput, calls=%fused_computation.16 | convolution fusion | flops 5925519360 | bytes 15748096 | tf_op jit(solution)/shard_map/dot_general | solution.py:487
  226.0 4.7 %fusion.2.x_ref = bf16[1024,1408]{1,0:T(8,128)(2,1)S(1)} fusion(f32[1026,1408]{1,0:T(8,128)S(1)} %fusion.6, f32[1026,1408]{1,0:T(8,128)S(1)} %copy-done.7, f32[1408]{0:T(1024)S(1)} %get-tuple-element.9, f32[1408]{0:T(1024)S(1)} %get-tuple-element.10, f32[1408]{0:T(1024)S(1)} %get-tuple-element.8, f32[1408]{0:T(1024)S(1)} %get-tuple-element.24, ...), kind=kLoop, calls=%fused_computation.3 | loop fusion | flops 23068672 | bytes 37520384 | tf_op jit(solution)/shard_map/convert_element_type | solution.py:502
  230.8 77.9 %all-gather.8.cloned.1.call-done.w_ref = bf16[1408,2048]{1,0:T(8,128)(2,1)} async-done(((bf16[1408,256]{1,0:T(8,128)(2,1)}), bf16[1408,2048]{1,0:T(8,128)(2,1)}) %all-gather.8.cloned.1.call-update) | async-done | bytes 5767184 | tf_op jit(solution)/shard_map/all_gather | solution.py:460
  308.7 2.6 copy-done.2
  311.3 28.4 %shard_map.157 = f32[256,2048]{1,0:T(8,128)S(1)} custom-call(bf16[1024,1408]{1,0:T(8,128)(2,1)S(1)} %fusion.2.x_ref, bf16[1408,2048]{1,0:T(8,128)(2,1)S(1)} %copy-done.2), custom_call_target="tpu_custom_call" | custom-call | flops 30000001024 | bytes 5767168 | tf_op jit(solution)/shard_map/pallas_call | solution.py:422
  339.8 1.3 fusion.11
  (60 shorter events, 4.2 us)
Async XLA Ops:
  6.5 8.4 %copy-start = (bf16[1024,256]{1,0:T(8,128)(2,1)S(1)}, bf16[1024,256]{1,0:T(8,128)(2,1)}, u32[]{:S(2)}) copy-start(bf16[1024,256]{1,0:T(8,128)(2,1)} %k_ref.1) | copy-start | bytes 1572868
  6.5 11.3 %copy-start.1 = (bf16[1024,512]{1,0:T(8,128)(2,1)S(1)}, bf16[1024,512]{1,0:T(8,128)(2,1)}, u32[]{:S(2)}) copy-start(bf16[1024,512]{1,0:T(8,128)(2,1)} %v_ref.1) | copy-start | bytes 3145732
  6.5 13.5 %copy-start.4 = (bf16[1024,512]{1,0:T(8,128)(2,1)S(1)}, bf16[1024,512]{1,0:T(8,128)(2,1)}, u32[]{:S(2)}) copy-start(bf16[1024,512]{1,0:T(8,128)(2,1)} %gate_ref.1) | copy-start | bytes 3145732
  6.5 13.5 %copy-start.6 = (f32[2,256]{1,0:T(2,128)S(1)}, f32[2,256]{1,0:T(2,128)}, u32[]{:S(2)}) copy-start(f32[2,256]{1,0:T(2,128)} %gain_ref.1) | copy-start | bytes 6148
  6.5 136.5 %all-gather.4.cloned.1.call-start = ((), (), s32[]{:S(2)}) async-start(), calls=%async_computation | async-start | bytes 6488064 | tf_op jit(solution)/shard_map/all_gather | solution.py:458
  7.3 208.0 %all-gather.6.cloned.1.call-start = ((), (), s32[]{:S(2)}) async-start(), calls=%async_computation.1 | async-start | bytes 6488064 | tf_op jit(solution)/shard_map/all_gather | solution.py:459
  8.0 300.7 %all-gather.8.cloned.1.call-start = ((), (), s32[]{:S(2)}) async-start(), calls=%async_computation.2 | async-start | bytes 6488064 | tf_op jit(solution)/shard_map/all_gather | solution.py:460
  20.1 1.1 copy-start.5
  21.2 57.5 %copy-start.3 = (bf16[512,2048]{1,0:T(8,128)(2,1)S(1)}, bf16[512,2048]{1,0:T(8,128)(2,1)}, u32[]{:S(2)}) copy-start(bf16[512,2048]{1,0:T(8,128)(2,1)} %w_ref.1) | copy-start | bytes 6291460
  78.8 27.8 %copy-start.10 = (bf16[256,2048]{1,0:T(8,128)(2,1)S(1)}, bf16[256,2048]{1,0:T(8,128)(2,1)}, u32[]{:S(2)}) copy-start(bf16[256,2048]{1,0:T(8,128)(2,1)} %param.16) | copy-start | bytes 3145732
  78.8 29.0 %copy-start.13 = (f32[2048]{0:T(1024)S(1)}, f32[2048]{0:T(1024)}, u32[]{:S(2)}) copy-start(f32[2048]{0:T(1024)} %param.26) | copy-start | bytes 24580
  106.8 1.0 copy-start.8
  108.1 31.3 %copy-start.11 = (f32[3,1408]{1,0:T(4,128)S(1)}, f32[3,1408]{1,0:T(4,128)}, u32[]{:S(2)}) copy-start(f32[3,1408]{1,0:T(4,128)} %param.30) | copy-start | bytes 50692
  108.1 31.3 %copy-start.12 = (f32[3,1408]{1,0:T(4,128)S(1)}, f32[3,1408]{1,0:T(4,128)}, u32[]{:S(2)}) copy-start(f32[3,1408]{1,0:T(4,128)} %param.29) | copy-start | bytes 50692
  138.0 5.1 %collective-permute-start = (bf16[2,2048]{1,0:T(2,128)(2,1)S(1)}, bf16[2,2048]{1,0:T(2,128)(2,1)S(1)}, u32[]{:S(2)}, u32[]{:S(2)}) collective-permute-start(bf16[2,2048]{1,0:T(2,128)(2,1)S(1)} %slice.44), channel_id=1, source_target_pairs={{0,4},{4,8},{8,12},{12,16},{16,20},{20,24},{24,28},{1,5},{5,9},{9,... | collective-permute-start | bytes 24584 | tf_op jit(solution)/shard_map/ppermute | solution.py:20
  215.3 10.7 %copy-start.7 = (f32[1026,1408]{1,0:T(8,128)S(1)}, f32[1026,1408]{1,0:T(8,128)}, u32[]{:S(2)}) copy-start(f32[1026,1408]{1,0:T(8,128)} %fusion.7) | copy-start | bytes 17335300
  308.7 2.6 copy-start.2
  311.3 28.4 %copy-start.9 = (bf16[256,2048]{1,0:T(8,128)(2,1)S(1)}, bf16[256,2048]{1,0:T(8,128)(2,1)}, u32[]{:S(2)}) copy-start(bf16[256,2048]{1,0:T(8,128)(2,1)} %copy-done.8) | copy-start | bytes 3145732
Sparse Core Ops, SparseCore 0:
  9.5 112.7 all-gather.3
  124.5 90.7 all-gather.5
  217.4 91.2 all-gather.7

commit v3 on v2

--- a/solution.py
+++ b/solution.py
@@ -434,6 +434,87 @@
     )(x, w)
 
 
+def walk_kernel(count, pieces, x_ref, out_ref, own_sem, send_sem, recv_sem):
+    me = lax.axis_index("sp")
+    odd = lax.rem(me, 2)
+    place = me // 2 + odd * (count - 1 - 2 * (me // 2))
+    size = x_ref.shape[0]
+    step = size // (2 * pieces)
+
+    def index(position):
+        position = lax.rem(position + 2 * count, count)
+        back = position // (count // 2)
+        return (1 - back) * 2 * position + back * (2 * (count - 1 - position) + 1)
+
+    ways = (1, -1)
+    barrier = pltpu.get_barrier_semaphore()
+    for way in ways:
+        pl.semaphore_signal(
+            barrier, inc=1, device_id={"sp": index(place + way)}, device_id_type=MESH
+        )
+    pl.semaphore_wait(barrier, 2)
+
+    def hop(w, t, p, age, own=False):
+        inner = (w * pieces + p) * step
+        owner = index(place - ways[w] * age)
+        dst = out_ref.at[pl.ds(pl.multiple_of(owner * size + inner, step), step)]
+        return pltpu.make_async_remote_copy(
+            src_ref=x_ref.at[pl.ds(inner, step)] if own else dst,
+            dst_ref=dst,
+            send_sem=send_sem.at[w, p, t],
+            recv_sem=recv_sem.at[w, p, t],
+            device_id={"sp": index(place + ways[w])},
+            device_id_type=MESH,
+        )
+
+    for p in range(pieces):
+        for w in range(2):
+            hop(w, 0, p, 0, True).start()
+    whole = pl.ds(pl.multiple_of(me * size, size), size)
+    own = pltpu.make_async_copy(x_ref, out_ref.at[whole], own_sem)
+    own.start()
+
+    @pl.loop(1, count - 1)
+    def _(t):
+        for p in range(pieces):
+            for w in range(2):
+                hop(w, t - 1, p, t).wait_recv()
+                hop(w, t, p, t).start()
+
+    own.wait()
+    for p in range(pieces):
+        for w in range(2):
+            hop(w, count - 2, p, count - 1).wait_recv()
+            hop(w, 0, p, 0, True).wait_send()
+
+    @pl.loop(1, count - 1)
+    def _(t):
+        for p in range(pieces):
+            for w in range(2):
+                hop(w, t, p, t).wait_send()
+
+
+def walk_gather(x, pieces):
+    count = lax.axis_size("sp")
+    if count % 2 or count < 4 or x.shape[0] % (32 * pieces):
+        return lax.all_gather(x, "sp", axis=0, tiled=True)
+    vmem = pl.BlockSpec(memory_space=pltpu.VMEM)
+    return pl.pallas_call(
+        functools.partial(walk_kernel, count, pieces),
+        out_shape=jax.ShapeDtypeStruct((count * x.shape[0], x.shape[1]), x.dtype),
+        in_specs=[vmem],
+        out_specs=vmem,
+        scratch_shapes=[pltpu.SemaphoreType.DMA]
+        + [pltpu.SemaphoreType.DMA((2, pieces, count - 1))] * 2,
+        compiler_params=pltpu.CompilerParams(
+            collective_id=4, has_side_effects=True, vmem_limit_bytes=16 * 1024 * 1024
+        ),
+        cost_estimate=pl.CostEstimate(
+            flops=30_000_000_000, bytes_accessed=count * x.size, transcendentals=0
+        ),
+    )(x)
+
+
 def local(
     residual_entry_input,
     query_matrix_rows,
@@ -456,7 +537,6 @@
         input_gate_logits, forget_gate_logits, forget_decay_offset
     )
     whole_gate = lax.all_gather(gate_up_weight, "sp", axis=0, tiled=True)
-    whole_value = lax.all_gather(value_up_weight, "sp", axis=0, tiled=True)
     whole_down = lax.all_gather(down_projection_weight, "sp", axis=1, tiled=True)
     gated_rows = cell(
         query_matrix_rows,
@@ -477,6 +557,8 @@
         * feedforward_norm_gain[None, :]
     ).astype(jnp.bfloat16)
     group_rows = gather_rows(normed_rows)
+    group_rows, value_shard = lax.optimization_barrier((group_rows, value_up_weight))
+    whole_value = walk_gather(value_shard, 2)
     earlier_rows = shifted(group_rows[-2:], "sp", 1)
     window = jnp.concatenate([earlier_rows, group_rows], axis=0)
     up_gate = jnp.dot(

time: 352 us -> 324 us (0.920); the launches traced: 348 us -> 323 us
  waiting for transfers between devices: 144 us -> 1.4 us
  Pallas kernels: 143 us -> 264 us
    pallas_call x0 -> x1, Pallas kernels: none -> 117 us  [walk_gather(): pl.pallas_call(functools.partial(walk_kernel, count, pieces), out_shape=j...]
    all_gather x1, waiting for transfers between devices: 77.9 us -> 0.02 us  [local(): lax.all_gather(down_projection_weight, 'sp', axis=1, tiled=True)]
    all_gather x1 -> x0, waiting for transfers between devices: 60.3 us -> none  [local(): whole_value = lax.all_gather(value_up_weight, 'sp', axis=0, tiled=True)]
    pallas_call x2, Pallas kernels: 56.1 us -> 63.1 us  [product_rows(): pl.pallas_call(functools.partial(product_kernel, pieces), out_shape=jax.S...]
  transfers between devices with their start and end apart: 4 -> 3, of which waited for: 3 -> 0; matrix products, arithmetic and copies ran while one was open for 12% -> 12% of each run, Pallas kernels for 33% -> 71%
where the time goes in v3:
time: 324 us; the launch traced here: 323 us
  Pallas kernels  264 us (81%)
  matrix products  21.4 us (7%)
  between operations  13.8 us (4%)
  local copies, waits for them, and re-layouts  10.8 us (3%)
  other arithmetic  10.2 us (3%)
    pallas_call x1, Pallas kernels, walk_gather(): pl.pallas_call(functools.partial(walk_kernel, count, pieces), out_shape=j...  117 us
    pallas_call x2, Pallas kernels, product_rows(): pl.pallas_call(functools.partial(product_kernel, pieces), out_shape=jax.S...  63.1 us
    pallas_call x1, Pallas kernels, cell(): pl.pallas_call(functools.partial(cell_kernel, count, heads), out_shape=ja...  57.3 us
    pallas_call x1, Pallas kernels, gather_rows(): pl.pallas_call(functools.partial(rows_kernel, pieces), out_shape=jax.Shap...  26.9 us
    dot_general x1, matrix products, local(): up_gate = jnp.dot(window, whole_gate, preferred_element_type=jnp.float32)  10.7 us
    dot_general x1, matrix products, local(): up_value = jnp.dot(window, whole_value, preferred_element_type=jnp.float32)  8.72 us
  transfers between devices with their start and end apart: 3, of which 0 were waited for; matrix products, arithmetic and copies ran while one was open for 12% of the time, Pallas kernels for 71%

profile of v3, /device:TPU:29, one launch (start us, length us, event | category | flops | bytes accessed | tf_op | source)
XLA Modules:
  0.0 323.2 jit_solution(9407974556567575655)
XLA Ops:
  6.6 0.7 all-gather.3.cloned.1.call-update
  7.3 0.7 all-gather.5.cloned.1.call-update
  8.0 0.7 fusion.22
  9.5 0.9 add_reduce_fusion
  10.5 1.1 mul.107
  11.6 2.5 copy.46
  14.2 2.2 copy.45
  16.4 1.4 multiply_reduce_fusion
  18.2 1.6 convolution_convert_fusion
  20.4 1.1 copy-done.7
  21.5 57.3 %shard_map.154.x_ref = bf16[1024,512]{1,0:T(8,128)(2,1)S(1)} custom-call(bf16[288,256]{1,0:T(8,128)(2,1)S(1)} %bitcast.46, bf16[1024,256]{1,0:T(8,128)(2,1)S(1)} %copy-done.7, bf16[1024,256]{1,0:T(8,128)(2,1)S(1)} %copy-done, bf16[1024,512]{1,0:T(8,128)(2,1)S(1)} %copy-done.1, bf16[1024,512]{1,0:T(8,128)(2,1)S(1)} %copy-done.5, f32[2,256]{1,0:T(2,128)S(1)} %copy-done.8, ...), custom_call_target="tpu_custom_call" | custom-call | flops 30000001024 | bytes 4194304 | tf_op jit(solution)/shard_map/pallas_call | solution.py:228
  78.8 27.8 %shard_map.155 = f32[256,2048]{1,0:T(8,128)S(1)} custom-call(bf16[1024,512]{1,0:T(8,128)(2,1)S(1)} %shard_map.154.x_ref, bf16[512,2048]{1,0:T(8,128)(2,1)S(1)} %copy-done.4), custom_call_target="tpu_custom_call" | custom-call | flops 30000001024 | bytes 2097152 | tf_op jit(solution)/shard_map/pallas_call | solution.py:422
  106.6 0.3 add_convert_fusion
  106.9 0.3 fusion.8
  107.2 0.3 fusion.10.x_ref
  107.5 26.9 %shard_map.156 = bf16[1024,2048]{1,0:T(8,128)(2,1)S(1)} custom-call(bf16[256,2048]{1,0:T(8,128)(2,1)S(1)} %fusion.10.x_ref), custom_call_target="tpu_custom_call" | custom-call | flops 30000001024 | bytes 2097152 | tf_op jit(solution)/shard_map/pallas_call | solution.py:310
  134.5 1.6 collective-permute-start
  136.1 116.7 %shard_map.157 = bf16[2048,1408]{1,0:T(8,128)(2,1)S(1)} custom-call(bf16[256,1408]{1,0:T(8,128)(2,1)S(1)} %copy-done.6), custom_call_target="tpu_custom_call" | custom-call | flops 30000001024 | bytes 2883584 | tf_op jit(solution)/shard_map/pallas_call | solution.py:502
  253.0 8.7 %fusion.6 = f32[1026,1408]{1,0:T(8,128)} fusion(bf16[2048,1408]{1,0:T(8,128)(2,1)S(1)} %shard_map.157, bf16[1024,2048]{1,0:T(8,128)(2,1)S(1)} %shard_map.156, bf16[2,2048]{1,0:T(2,128)(2,1)S(1)} %collective-permute-done), kind=kOutput, calls=%fused_computation.16 | convolution fusion | flops 5925519360 | bytes 15748096 | tf_op jit(solution)/shard_map/dot_general | solution.py:569
  261.7 10.7 %fusion.7 = f32[1026,1408]{1,0:T(8,128)S(1)} fusion(bf16[2048,1408]{1,0:T(8,128)(2,1)} %all-gather.3.cloned.1.call-done, bf16[1024,2048]{1,0:T(8,128)(2,1)} %copy-done.2, bf16[2,2048]{1,0:T(2,128)(2,1)S(1)} %collective-permute-done), kind=kOutput, calls=%fused_computation.17 | convolution fusion | flops 5925519360 | bytes 15748096 | tf_op jit(solution)/shard_map/dot_general | solution.py:564
  272.4 4.7 %fusion.2.x_ref = bf16[1024,1408]{1,0:T(8,128)(2,1)S(1)} fusion(f32[1026,1408]{1,0:T(8,128)S(1)} %copy-done.9, f32[1026,1408]{1,0:T(8,128)S(1)} %fusion.7, f32[1408]{0:T(1024)S(1)} %get-tuple-element.13, f32[1408]{0:T(1024)S(1)} %get-tuple-element.14, f32[1408]{0:T(1024)S(1)} %get-tuple-element.12, f32[1408]{0:T(1024)S(1)} %get-tuple-element.28, ...), kind=kLoop, calls=%fused_computation.3 | loop fusion | flops 23068672 | bytes 37520384 | tf_op jit(solution)/shard_map/convert_element_type | solution.py:584
  277.1 2.6 copy-done.3
  279.8 35.3 %shard_map.158 = f32[256,2048]{1,0:T(8,128)S(1)} custom-call(bf16[1024,1408]{1,0:T(8,128)(2,1)S(1)} %fusion.2.x_ref, bf16[1408,2048]{1,0:T(8,128)(2,1)S(1)} %copy-done.3), custom_call_target="tpu_custom_call" | custom-call | flops 30000001024 | bytes 5767168 | tf_op jit(solution)/shard_map/pallas_call | solution.py:422
  315.1 1.3 fusion.11
  (62 shorter events, 2.0 us)
Async XLA Ops:
  6.5 9.9 %copy-start = (bf16[1024,256]{1,0:T(8,128)(2,1)S(1)}, bf16[1024,256]{1,0:T(8,128)(2,1)}, u32[]{:S(2)}) copy-start(bf16[1024,256]{1,0:T(8,128)(2,1)} %k_ref.1) | copy-start | bytes 1572868
  6.5 11.6 %copy-start.1 = (bf16[1024,512]{1,0:T(8,128)(2,1)S(1)}, bf16[1024,512]{1,0:T(8,128)(2,1)}, u32[]{:S(2)}) copy-start(bf16[1024,512]{1,0:T(8,128)(2,1)} %v_ref.1) | copy-start | bytes 3145732
  6.5 13.8 %copy-start.5 = (bf16[1024,512]{1,0:T(8,128)(2,1)S(1)}, bf16[1024,512]{1,0:T(8,128)(2,1)}, u32[]{:S(2)}) copy-start(bf16[1024,512]{1,0:T(8,128)(2,1)} %gate_ref.1) | copy-start | bytes 3145732
  6.5 13.9 %copy-start.8 = (f32[2,256]{1,0:T(2,128)S(1)}, f32[2,256]{1,0:T(2,128)}, u32[]{:S(2)}) copy-start(f32[2,256]{1,0:T(2,128)} %gain_ref.1) | copy-start | bytes 6148
  6.5 255.1 %all-gather.3.cloned.1.call-start = ((), (), s32[]{:S(2)}) async-start(), calls=%async_computation | async-start | bytes 6488064 | tf_op jit(solution)/shard_map/all_gather | solution.py:539
  7.3 269.8 %all-gather.5.cloned.1.call-start = ((), (), s32[]{:S(2)}) async-start(), calls=%async_computation.1 | async-start | bytes 6488064 | tf_op jit(solution)/shard_map/all_gather | solution.py:540
  20.4 1.1 copy-start.7
  21.5 57.3 %copy-start.4 = (bf16[512,2048]{1,0:T(8,128)(2,1)S(1)}, bf16[512,2048]{1,0:T(8,128)(2,1)}, u32[]{:S(2)}) copy-start(bf16[512,2048]{1,0:T(8,128)(2,1)} %w_ref.1) | copy-start | bytes 6291460
  78.8 27.8 %copy-start.12 = (bf16[256,2048]{1,0:T(8,128)(2,1)S(1)}, bf16[256,2048]{1,0:T(8,128)(2,1)}, u32[]{:S(2)}) copy-start(bf16[256,2048]{1,0:T(8,128)(2,1)} %param.16) | copy-start | bytes 3145732
  78.8 28.4 %copy-start.15 = (f32[2048]{0:T(1024)S(1)}, f32[2048]{0:T(1024)}, u32[]{:S(2)}) copy-start(f32[2048]{0:T(1024)} %param.26) | copy-start | bytes 24580
  106.9 27.5 %copy-start.10 = (bf16[256,2048]{1,0:T(8,128)(2,1)}, bf16[256,2048]{1,0:T(8,128)(2,1)S(1)}, u32[]{:S(2)}) copy-start(bf16[256,2048]{1,0:T(8,128)(2,1)S(1)} %add_convert_fusion) | copy-start | bytes 3145732
  107.5 28.6 %copy-start.6 = (bf16[256,1408]{1,0:T(8,128)(2,1)S(1)}, bf16[256,1408]{1,0:T(8,128)(2,1)}, u32[]{:S(2)}) copy-start(bf16[256,1408]{1,0:T(8,128)(2,1)} %x_ref) | copy-start | bytes 2162692
  134.4 118.5 %copy-start.2 = (bf16[1024,2048]{1,0:T(8,128)(2,1)}, bf16[1024,2048]{1,0:T(8,128)(2,1)S(1)}, u32[]{:S(2)}) copy-start(bf16[1024,2048]{1,0:T(8,128)(2,1)S(1)} %shard_map.156) | copy-start | bytes 12582916
  134.4 118.4 %copy-start.13 = (f32[3,1408]{1,0:T(4,128)S(1)}, f32[3,1408]{1,0:T(4,128)}, u32[]{:S(2)}) copy-start(f32[3,1408]{1,0:T(4,128)} %param.30) | copy-start | bytes 50692
  134.4 118.4 %copy-start.14 = (f32[3,1408]{1,0:T(4,128)S(1)}, f32[3,1408]{1,0:T(4,128)}, u32[]{:S(2)}) copy-start(f32[3,1408]{1,0:T(4,128)} %param.29) | copy-start | bytes 50692
  134.5 118.5 %collective-permute-start = (bf16[2,2048]{1,0:T(2,128)(2,1)S(1)}, bf16[2,2048]{1,0:T(2,128)(2,1)S(1)}, u32[]{:S(2)}, u32[]{:S(2)}) collective-permute-start(bf16[2,2048]{1,0:T(2,128)(2,1)S(1)} %slice.44), channel_id=1, source_target_pairs={{0,4},{4,8},{8,12},{12,16},{16,20},{20,24},{24,28},{1,5},{5,9},{9,... | collective-permute-start | bytes 24584 | tf_op jit(solution)/shard_map/ppermute | solution.py:20
  261.7 10.7 %copy-start.9 = (f32[1026,1408]{1,0:T(8,128)S(1)}, f32[1026,1408]{1,0:T(8,128)}, u32[]{:S(2)}) copy-start(f32[1026,1408]{1,0:T(8,128)} %fusion.6) | copy-start | bytes 17335300
  277.1 2.6 copy-start.3
  279.8 35.3 %copy-start.11 = (bf16[256,2048]{1,0:T(8,128)(2,1)S(1)}, bf16[256,2048]{1,0:T(8,128)(2,1)}, u32[]{:S(2)}) copy-start(bf16[256,2048]{1,0:T(8,128)(2,1)} %copy-done.10) | copy-start | bytes 3145732
Sparse Core Ops, SparseCore 0:
  9.5 112.5 all-gather.2
  124.2 135.3 all-gather.4
